TPU v7x, 32 devices: a whole 2x2x4 slice. The times are simulated.
32 devices in a mesh: rep: 2 (over x), fs: 8 (over z, y), tp: 2 (over core).
Axes of the slice: x: 2, y: 2, z: 4, core: 2. Of those that a mesh axis runs over, the one named last changes fastest.
Arguments:
- tokens: bfloat16 [6144, 2048], P(('rep', 'fs')), may hold values from -6 to 6
- first_gain: float32 [2048], replicated, may hold values from 0.1 to 1.9
- mixer_gate: bfloat16 [2048, 2048], P('fs', 'tp'), may hold values from -0.125 to 0.125
- mixer_value: bfloat16 [2048, 2048], P('fs', 'tp'), may hold values from -1 to 1
- value_gain: float32 [2048], replicated, may hold values from 0.1 to 1.9
- value_shift: float32 [2048], replicated, may hold values from -3 to 3
- spatial_weight: bfloat16 [16, 128, 128], replicated, may hold values from -0.75 to 0.75
- spatial_bias: float32 [16, 128], replicated, may hold values from 0.1 to 1.9
- mixer_out: bfloat16 [2048, 2048], P('tp', 'fs'), may hold values from -0.125 to 0.125
- second_gain: float32 [2048], replicated, may hold values from 0.1 to 1.9
- up_gate: bfloat16 [2048, 4096], P('fs', 'tp'), may hold values from -0.125 to 0.125
- up_value: bfloat16 [2048, 4096], P('fs', 'tp'), may hold values from -0.125 to 0.125
- taps_gate: float32 [3, 4096], replicated, may hold values from -3.5 to 3.5
- taps_value: float32 [3, 4096], replicated, may hold values from -3.5 to 3.5
- down_proj: bfloat16 [4096, 2048], P('tp', 'fs'), may hold values from -0.09375 to 0.09375
Outputs:
- layer_out: bfloat16 [6144, 2048], P(('rep', 'fs'))
All inputs are finite; a program needn't handle non-finite values.
Results may differ from a plain program's by a relative error of at most 0.015.
Values may be sent and summed in bfloat16 or wider, within the bound.
A program may use at most 64 MiB of HBM per device.

v0:
```python
import functools

import jax
import jax.numpy as jnp
from jax import lax
from jax.experimental import pallas as pl
from jax.experimental.pallas import tpu as pltpu
from jax.sharding import PartitionSpec as P

D = 2048
GDIM = 128
BLK = 128
LEN = 128


def normalize(matrix, scale_gain):
    values = matrix.astype(jnp.float32)
    factor = lax.rsqrt(jnp.mean(values * values, axis=-1, keepdims=True) + 1e-06)
    return (values * factor * scale_gain).astype(jnp.bfloat16)


def causal_conv(values, tap_weights):
    by_sequence = values.reshape(-1, LEN, values.shape[-1])
    padded = jnp.pad(by_sequence, ((0, 0), (2, 0), (0, 0)))
    summed = (
        tap_weights[0] * padded[:, 0:LEN]
        + tap_weights[1] * padded[:, 1 : LEN + 1]
        + tap_weights[2] * padded[:, 2 : LEN + 2]
    )
    return summed.reshape(values.shape)


def local(
    tokens,
    first_gain,
    mixer_gate,
    mixer_value,
    value_gain,
    value_shift,
    spatial_weight,
    spatial_bias,
    mixer_out,
    second_gain,
    up_gate,
    up_value,
    taps_gate,
    taps_value,
    down_proj,
):
    n_rep, n_tp = lax.axis_size("rep"), lax.axis_size("tp")
    rep_index, tp_index = lax.axis_index("rep"), lax.axis_index("tp")
    team = ("rep", "tp")

    def part(array, axis):
        width = array.shape[axis] // n_rep
        return lax.dynamic_slice_in_dim(array, rep_index * width, width, axis)

    def own(array, width, axis):
        at = (tp_index * n_rep + rep_index) * width
        return lax.dynamic_slice_in_dim(array, at, width, axis)

    w_gate = lax.all_gather(part(mixer_gate, 1), "fs", axis=0, tiled=True)
    w_value = lax.all_gather(part(mixer_value, 1), "fs", axis=0, tiled=True)
    w_out = lax.all_gather(part(mixer_out, 0), "fs", axis=1, tiled=True)
    u_gate = lax.all_gather(part(up_gate, 1), "fs", axis=0, tiled=True)
    u_value = lax.all_gather(part(up_value, 1), "fs", axis=0, tiled=True)
    w_down = lax.all_gather(part(down_proj, 0), "fs", axis=1, tiled=True)

    row_share = tokens.shape[0] // n_tp
    kept_tokens = lax.dynamic_slice_in_dim(tokens, tp_index * row_share, row_share, 0)
    first = lax.all_gather(normalize(kept_tokens, first_gain), team, axis=0, tiled=True)
    row_count = first.shape[0]
    cols = w_gate.shape[1]
    gate_act = jax.nn.gelu(jnp.dot(first, w_gate, preferred_element_type=jnp.float32))
    value_act = jax.nn.gelu(jnp.dot(first, w_value, preferred_element_type=jnp.float32))
    value_sum, value_squares = lax.psum(
        (jnp.sum(value_act, axis=1), jnp.sum(value_act * value_act, axis=1)), team
    )
    row_mean = value_sum / D
    variance = value_squares / D - row_mean * row_mean
    centred = (
        (value_act - row_mean[:, None])
        * lax.rsqrt(variance[:, None] + 1e-05)
        * own(value_gain, cols, 0)
        + own(value_shift, cols, 0)
    ).astype(jnp.bfloat16)
    groups = cols // GDIM
    masked = own(spatial_weight, groups, 0) * jnp.tril(jnp.ones((BLK, BLK), jnp.bfloat16))
    blocks = centred.reshape(row_count // BLK, BLK, groups, GDIM)
    mixed_rows = (
        jnp.einsum("gts,bsgc->btgc", masked, blocks, preferred_element_type=jnp.float32)
        + own(spatial_bias, groups, 0).T[None, :, :, None]
    )
    gated_rows = (gate_act * mixed_rows.reshape(row_count, cols)).astype(jnp.bfloat16)
    summed = lax.psum_scatter(
        jnp.dot(gated_rows, w_out, preferred_element_type=jnp.float32).astype(jnp.bfloat16),
        team,
        scatter_dimension=0,
        tiled=True,
    ).astype(jnp.float32)
    residual = (kept_tokens.astype(jnp.float32) + summed).astype(jnp.bfloat16)
    second = lax.all_gather(normalize(residual, second_gain), team, axis=0, tiled=True)
    hidden_cols = u_gate.shape[1]
    gate_up = jnp.dot(second, u_gate, preferred_element_type=jnp.float32)
    value_up = jnp.dot(second, u_value, preferred_element_type=jnp.float32)
    hidden = (
        jax.nn.silu(causal_conv(gate_up, own(taps_gate, hidden_cols, 1)))
        * causal_conv(value_up, own(taps_value, hidden_cols, 1))
    ).astype(jnp.bfloat16)
    ffn_total = lax.psum_scatter(
        jnp.dot(hidden, w_down, preferred_element_type=jnp.float32).astype(jnp.bfloat16),
        team,
        scatter_dimension=0,
        tiled=True,
    ).astype(jnp.float32)
    final_rows = (residual.astype(jnp.float32) + ffn_total).astype(jnp.bfloat16)
    return lax.all_gather(final_rows, "tp", axis=0, tiled=True)


PLANE = 2
ARRAYS = 6
FAR = 3
MESH = pl.DeviceIdType.MESH


def team_kernel(
    dims,
    tokens,
    first_gain,
    mixer_gate,
    mixer_value,
    value_gain,
    value_shift,
    spatial_weight,
    spatial_bias,
    mixer_out,
    second_gain,
    up_gate,
    up_value,
    taps_gate,
    taps_value,
    down_proj,
    out,
    w_gate,
    w_value,
    w_out,
    w_ug,
    w_uv,
    w_down,
    tok,
    rows_in,
    gate_act,
    value_act,
    gated,
    gate_half,
    hidden,
    part,
    from_partner,
    from_team,
    residual,
    stats,
    own_sem,
    side_send,
    up_send,
    down_send,
    weight_recv,
    team_send,
    team_recv,
    pass_send,
    pass_recv,
    stat_send,
    stat_recv,
    pair_send,
    pair_recv,
    sum_send,
    sum_recv,
    cross_send,
    cross_recv,
    last_sem,
):
    n_rep, n_fs, n_tp = dims
    n_side, n_line = PLANE, n_fs // PLANE
    n_chip = n_rep * n_side
    x, c = lax.axis_index("rep"), lax.axis_index("tp")
    f_own = lax.axis_index("fs")
    z, y = f_own // n_side, f_own % n_side
    other = (c + 1) % n_tp
    q_own = x * n_side + y
    rows = tokens.shape[0]
    half = rows // n_tp
    width = tokens.shape[1]
    sources = (mixer_gate, mixer_value, mixer_out, up_gate, up_value, down_proj)
    held = (w_gate, w_value, w_out, w_ug, w_uv, w_down)
    offsets = [(dx, dy) for dx in range(n_rep) for dy in range(n_side)]
    partner = (x, f_own, other)

    def chip_to(k, core):
        dx, dy = offsets[k]
        return ((x + dx) % n_rep, z * n_side + (y + dy) % n_side, core)

    def chip_q(k, sign):
        dx, dy = offsets[k]
        return ((x + sign * dx + n_rep) % n_rep) * n_side + (y + sign * dy + n_side) % n_side

    def remote(src, dst, send, recv, device):
        return pltpu.make_async_remote_copy(
            src_ref=src, dst_ref=dst, send_sem=send, recv_sem=recv, device_id=device, device_id_type=MESH
        )

    def block(a, f):
        if len(held[a].shape) == 3:
            return held[a].at[f]
        height = sources[a].shape[0]
        return held[a].at[pl.ds(pl.multiple_of(f * height, height), height)]

    def piece(a, q):
        if len(held[a].shape) == 3:
            height = sources[a].shape[0] // n_chip
            return sources[a].at[pl.ds(pl.multiple_of(q * height, height), height)]
        cols = sources[a].shape[1] // n_chip
        return sources[a].at[:, pl.ds(pl.multiple_of(q * cols, cols), cols)]

    def own_copy(a):
        return pltpu.make_async_copy(piece(a, q_own), block(a, f_own), own_sem.at[a])

    def side(a, dy):
        to_y = (y + dy) % n_side
        return remote(
            piece(a, x * n_side + to_y),
            block(a, f_own),
            side_send.at[a, dy],
            weight_recv.at[a, f_own],
            (x, z * n_side + to_y, c),
        )

    def along(a, f, step, src):
        sem = up_send if step == 1 else down_send
        return remote(
            src, block(a, f), sem.at[a, f], weight_recv.at[a, f], (x, f_own + step * n_side, c)
        )

    def landed(a, f):
        remote(block(a, f), block(a, f), side_send.at[a, 0], weight_recv.at[a, f], partner).wait_recv()

    has_up, has_down = z + 1 < n_line, z >= 1

    def send_line(a, f, src, up=True, down=True):
        if up:
            pl.when(has_up)(lambda: along(a, f, 1, src).start())
        if down:
            pl.when(has_down)(lambda: along(a, f, -1, src).start())

    def start_side(a):
        own_copy(a).start()
        for dy in range(1, n_side):
            side(a, dy).start()

    def start_line(a):
        send_line(a, f_own, piece(a, q_own))

    def relay(a, d):
        if d == 0:
            for dy in range(1, n_side):
                f = z * n_side + (y + dy) % n_side
                landed(a, f)
                send_line(a, f, block(a, f))
            own_copy(a).wait()
            return
        for j in range(n_side):

            @pl.when(z - d >= 0)
            def _():
                f = (z - d) * n_side + j
                landed(a, f)
                send_line(a, f, block(a, f), down=False)

            @pl.when(z + d < n_line)
            def _():
                f = (z + d) * n_side + j
                landed(a, f)
                send_line(a, f, block(a, f), up=False)

    def chip_rows(q, core):
        return pl.ds(pl.multiple_of(q * rows + core * half, half), half)

    def share(g, k, buffer, src):
        place = buffer.at[chip_rows(q_own, c)]
        return remote(src, place, team_send.at[g, k], team_recv.at[g, k], chip_to(k, c))

    def share_landed(g, k, buffer):
        place = buffer.at[chip_rows(chip_q(k, -1), c)]
        remote(place, place, team_send.at[g, k], team_recv.at[g, k], partner).wait_recv()

    def across_place(buffer, q, k):
        quarter = half // 2
        first = q * rows + c * half + (quarter if k == 1 else 0)
        return buffer.at[pl.ds(pl.multiple_of(first, quarter), quarter)]

    def across(g, k, buffer):
        place = across_place(buffer, chip_q(k, -1), k)
        return remote(
            place, place, cross_send.at[g, k], cross_recv.at[g, k], chip_to(FAR - k, c)
        )

    def across_landed(g, k, buffer):
        place = across_place(buffer, chip_q(FAR, -1), k)
        remote(place, place, cross_send.at[g, k], cross_recv.at[g, k], partner).wait_recv()

    def hand_on(g, k, buffer):
        place = buffer.at[chip_rows(chip_q(k, -1), c)]
        return remote(place, place, pass_send.at[g, k], pass_recv.at[g, k], partner)

    def hand_landed(g, k, buffer):
        place = buffer.at[chip_rows(chip_q(k, -1), other)]
        remote(place, place, pass_send.at[g, k], pass_recv.at[g, k], partner).wait_recv()

    def norm_rows(values, gain):
        factor = lax.rsqrt(jnp.mean(values * values, axis=-1, keepdims=True) + 1e-06)
        return (values * factor * gain).astype(jnp.bfloat16)

    step_rows = 64

    def norm_chip(q):
        def body(i, carry):
            at = pl.ds(pl.multiple_of(q * rows + i * step_rows, step_rows), step_rows)
            rows_in[at, :] = norm_rows(tok[at, :].astype(jnp.float32), first_gain[...])
            return carry

        lax.fori_loop(0, rows // step_rows, body, 0)

    barrier = pltpu.get_barrier_semaphore()
    for k in range(n_chip):
        for core in (c, other):
            if k or core is other:
                pl.semaphore_signal(barrier, inc=1, device_id=chip_to(k, core), device_id_type=MESH)
    for flag, step in ((has_up, 1), (has_down, -1)):

        @pl.when(flag)
        def _():
            pl.semaphore_signal(
                barrier, inc=1, device_id=(x, f_own + step * n_side, c), device_id_type=MESH
            )

    neighbours = has_up.astype(jnp.int32) + has_down.astype(jnp.int32)
    pl.semaphore_wait(barrier, n_chip * n_tp - 1 + neighbours)

    my_tokens = tokens.at[pl.ds(pl.multiple_of(c * half, half), half)]
    for a in range(3):
        start_side(a)
    start_line(0)
    start_line(1)
    for k in (1, 2):
        share(0, k, tok, my_tokens).start()
    tok_copy = pltpu.make_async_copy(
        tokens, tok.at[pl.ds(pl.multiple_of(q_own * rows, rows), rows)], own_sem.at[ARRAYS]
    )
    tok_copy.start()
    for a in range(3, ARRAYS):
        start_side(a)
    relay(0, 0)
    relay(1, 0)
    for d in range(1, n_line):
        relay(0, d)
    start_line(2)
    relay(2, 0)
    tok_copy.wait()
    norm_chip(q_own)
    for k in (1, 2):
        share_landed(0, k, tok)
        across(0, k, tok).start()
        hand_on(0, k, tok).start()
    for d in range(1, n_line):
        relay(1, d)
    start_line(3)
    relay(3, 0)
    for k in (1, 2):
        across_landed(0, k, tok)
    hand_on(0, FAR, tok).start()
    relay(2, 1)
    for k in range(1, n_chip):
        hand_landed(0, k, tok)
        norm_chip(chip_q(k, -1))
    for d in range(2, n_line - 1):
        relay(2, d)

    def project(weight, target):
        tile = half

        def body(i, carry):
            at = pl.ds(pl.multiple_of(i * tile, tile), tile)
            product = jnp.dot(rows_in[at, :], weight[...], preferred_element_type=jnp.float32)
            target[at, :] = jax.nn.gelu(product)
            return carry

        lax.fori_loop(0, n_chip * n_tp, body, 0)

    cols = w_gate.shape[1]
    slot = c * n_chip + q_own
    blocks = n_chip * rows // BLK
    lane = lax.broadcasted_iota(jnp.int32, (BLK, BLK), 1)
    sub = lax.broadcasted_iota(jnp.int32, (BLK, BLK), 0)
    project(w_value, value_act)

    def stat_body(i, carry):
        at = pl.ds(pl.multiple_of(i * BLK, BLK), BLK)
        values = value_act[at, :]
        total = jnp.sum(values, axis=1, keepdims=True)
        squares = jnp.sum(values * values, axis=1, keepdims=True)
        both = jnp.where(lane == 0, total, squares).T
        stats[0, :, at] = both[0:2, :]
        return carry

    lax.fori_loop(0, blocks, stat_body, 0)
    mates = [(k, j) for k in range(n_chip) for j in range(n_tp) if k or j]

    def tell(i):
        k, j = mates[i]
        return remote(
            stats.at[0],
            stats.at[i + 1],
            stat_send.at[i],
            stat_recv.at[i],
            chip_to(k, (c + j) % n_tp),
        )

    for i in range(len(mates)):
        tell(i).start()
    project(w_gate, gate_act)
    for d in range(max(2, n_line - 1), n_line):
        relay(2, d)
    start_line(4)
    relay(4, 0)
    for i in range(len(mates)):
        tell(i).wait_recv()
    at_cols = pl.ds(pl.multiple_of(slot * cols, cols), cols)
    groups = cols // GDIM

    def mix_body(i, carry):
        at = pl.ds(pl.multiple_of(i * BLK, BLK), BLK)
        total = stats[0, :, at]
        for s in range(1, len(mates) + 1):
            total = total + stats[s, :, at]
        row_mean = jnp.broadcast_to(total[0:1, :] / width, (BLK, BLK)).T[:, 0:1]
        row_square = jnp.broadcast_to(total[1:2, :] / width, (BLK, BLK)).T[:, 0:1]
        variance = row_square - row_mean * row_mean
        centred = (
            (value_act[at, :] - row_mean) * lax.rsqrt(variance + 1e-05) * value_gain[:, at_cols]
            + value_shift[:, at_cols]
        ).astype(jnp.bfloat16)
        for g in range(groups):
            group = slot * groups + g
            matrix = spatial_weight[group]
            matrix = jnp.where(sub >= lane, matrix, jnp.zeros_like(matrix))
            bias = jnp.broadcast_to(spatial_bias[pl.ds(group, 1), :], (BLK, BLK)).T
            mixed = (
                jnp.dot(
                    matrix, centred[:, g * GDIM : (g + 1) * GDIM], preferred_element_type=jnp.float32
                )
                + bias
            )
            channels = slice(g * GDIM, (g + 1) * GDIM)
            gated[at, channels] = (gate_act[at, channels] * mixed).astype(jnp.bfloat16)
        return carry

    lax.fori_loop(0, blocks, mix_body, 0)

    out_width = w_out.shape[2] * n_side

    def plane_cols(p):
        return pl.ds(pl.multiple_of(p * out_width, out_width), out_width)

    def pair(s, p, q):
        place = plane_cols(p)
        return remote(
            part.at[chip_rows(q, other), place],
            from_partner.at[pl.ds(pl.multiple_of(q * half, half), half), place],
            pair_send.at[s, p, q],
            pair_recv.at[s, p, q],
            partner,
        )

    def piece_cols(p, j):
        cut = w_out.shape[2]
        return pl.ds(pl.multiple_of((p * n_side + j) * cut, cut), cut)

    def to_team(s, p, j, t):
        near = 2 if j == 0 else 1
        place = piece_cols(p, j)
        k_rows = (near, FAR, FAR - near)[t]
        k_chip = (near, near, FAR - near)[t]
        return remote(
            part.at[chip_rows(chip_q(k_rows, 1), c), place],
            from_team.at[t, :, place],
            sum_send.at[s, p, j * FAR + t],
            sum_recv.at[s, p, j * FAR + t],
            chip_to(k_chip, c),
        )

    def out_plane(s, p, acts, weight):
        def multiply(q, carry):
            at = pl.ds(pl.multiple_of(q * rows, rows), rows)
            for j in range(n_side):
                part[at, piece_cols(p, j)] = jnp.dot(
                    acts[at, :], weight[p * n_side + j], preferred_element_type=jnp.float32
                ).astype(jnp.bfloat16)
            pair(s, p, q).start()
            return carry

        lax.fori_loop(0, n_chip, multiply, 0)
        place = plane_cols(p)
        for k in (3, 2, 1, 0):
            q = chip_q(k, 1)
            pair(s, p, q).wait_recv()
            at = chip_rows(q, c)
            part[at, place] = (
                part[at, place].astype(jnp.float32)
                + from_partner[pl.ds(pl.multiple_of(q * half, half), half), place].astype(
                    jnp.float32
                )
            ).astype(jnp.bfloat16)
            for j in range(n_side):
                if k == FAR:
                    to_team(s, p, j, 1).start()
                elif k == 2 - j:
                    to_team(s, p, j, 0).start()

    def pass_plane(s, p):
        for j in range(n_side):
            to_team(s, p, j, 1).wait_recv()
            at, place = chip_rows(chip_q(1 if j == 0 else 2, 1), c), piece_cols(p, j)
            part[at, place] = (
                part[at, place].astype(jnp.float32) + from_team[1, :, place].astype(jnp.float32)
            ).astype(jnp.bfloat16)
            to_team(s, p, j, 2).start()

    def finish_plane(s, p, carry):
        for j in range(n_side):
            to_team(s, p, j, 0).wait_recv()
            to_team(s, p, j, 2).wait_recv()
        return carry

    def drain_plane(s, p, carry):
        for j in range(n_side):
            for t in range(FAR):
                to_team(s, p, j, t).wait_send()
        for q in range(n_chip):
            pair(s, p, q).wait_send()
        return carry

    def summed(i):
        at = pl.ds(pl.multiple_of(i * step_rows, step_rows), step_rows)
        mine = pl.ds(pl.multiple_of(q_own * rows + c * half + i * step_rows, step_rows), step_rows)
        total = part[mine, :].astype(jnp.float32)
        for t in (0, 2):
            total = total + from_team[t, at, :].astype(jnp.float32)
        return at, mine, total

    def out_body(p, carry):
        out_plane(0, p, gated, w_out)
        return carry

    def pass_body(p, carry):
        pass_plane(0, p)
        return carry

    lax.fori_loop(0, n_line, out_body, 0)
    relay(3, 1)
    lax.fori_loop(0, n_line, pass_body, 0)
    for d in range(2, n_line):
        relay(3, d)
    start_line(5)
    lax.fori_loop(0, n_line, functools.partial(finish_plane, 0), 0)

    def residual_body(i, carry):
        at, mine, total = summed(i)
        kept = (tok[mine, :].astype(jnp.float32) + total).astype(jnp.bfloat16)
        residual[at, :] = kept
        rows_in[mine, :] = norm_rows(kept.astype(jnp.float32), second_gain[...])
        return carry

    lax.fori_loop(0, half // step_rows, residual_body, 0)
    mine = rows_in.at[chip_rows(q_own, c)]
    for k in (1, 2):
        share(1, k, rows_in, mine).start()
    hand_on(1, 0, rows_in).start()
    relay(5, 0)
    lax.fori_loop(0, n_line, functools.partial(drain_plane, 0), 0)
    relay(4, 1)
    for k in (1, 2):
        share_landed(1, k, rows_in)
        across(1, k, rows_in).start()
        hand_on(1, k, rows_in).start()
    for d in range(2, n_line):
        relay(4, d)
    for k in (1, 2):
        across_landed(1, k, rows_in)
    hand_on(1, FAR, rows_in).start()
    for k in range(n_chip):
        hand_landed(1, k, rows_in)

    hidden_cols = w_ug.shape[1]
    at_hidden = pl.ds(pl.multiple_of(slot * hidden_cols, hidden_cols), hidden_cols)
    position = lax.broadcasted_iota(jnp.int32, (LEN, hidden_cols), 0)

    def conv(values, taps):
        back1 = jnp.where(position >= 1, pltpu.roll(values, 1, 0), 0.0)
        back2 = jnp.where(position >= 2, pltpu.roll(values, 2, 0), 0.0)
        weights = taps[:, at_hidden]
        return weights[0:1] * back2 + weights[1:2] * back1 + weights[2:3] * values

    def raise_body(weight, taps, last, i, carry):
        at = pl.ds(pl.multiple_of(i * rows, rows), rows)
        product = jnp.dot(rows_in[at, :], weight[...], preferred_element_type=jnp.float32)
        for s in range(rows // LEN):
            here = pl.ds(pl.multiple_of(i * rows + s * LEN, LEN), LEN)
            done = conv(product[s * LEN : (s + 1) * LEN], taps)
            if last:
                hidden[here, :] = (gate_half[here, :] * done).astype(jnp.bfloat16)
            else:
                gate_half[here, :] = jax.nn.silu(done)
        return carry

    lax.fori_loop(0, n_chip, functools.partial(raise_body, w_ug, taps_gate, False), 0)
    relay(5, 1)
    lax.fori_loop(0, n_chip, functools.partial(raise_body, w_uv, taps_value, True), 0)

    def at_distance(d, act):
        pl.when(z - d >= 0)(lambda: act(z - d))
        if d:
            pl.when(z + d < n_line)(lambda: act(z + d))

    for d in range(n_line):
        if d > 1:
            relay(5, d)
        at_distance(d, lambda p: out_plane(1, p, hidden, w_down))
        if d:
            at_distance(d - 1, lambda p: pass_plane(1, p))
    at_distance(n_line - 1, lambda p: pass_plane(1, p))
    lax.fori_loop(0, n_line, functools.partial(finish_plane, 1), 0)

    def last_body(i, carry):
        at, mine, total = summed(i)
        here = pl.ds(pl.multiple_of(c * half + i * step_rows, step_rows), step_rows)
        out[here, :] = (residual[at, :].astype(jnp.float32) + total).astype(jnp.bfloat16)
        return carry

    lax.fori_loop(0, half // step_rows, last_body, 0)
    my_half = out.at[pl.ds(pl.multiple_of(c * half, half), half)]
    last = remote(my_half, my_half, last_sem.at[0], last_sem.at[1], partner)
    last.start()
    lax.fori_loop(0, n_line, functools.partial(drain_plane, 1), 0)
    for i in range(len(mates)):
        tell(i).wait_send()
    for k in (1, 2):
        share(0, k, tok, my_tokens).wait_send()
        share(1, k, rows_in, mine).wait_send()
        across(0, k, tok).wait_send()
        across(1, k, rows_in).wait_send()
    for k in range(1, n_chip):
        hand_on(0, k, tok).wait_send()
    for k in range(n_chip):
        hand_on(1, k, rows_in).wait_send()
    for a in range(ARRAYS):
        for dy in range(1, n_side):
            side(a, dy).wait_send()

        def settle(f, carry, a=a):
            @pl.when(has_up & (f // n_side <= z))
            def _():
                along(a, f, 1, block(a, f)).wait_send()

            @pl.when(has_down & (f // n_side >= z))
            def _():
                along(a, f, -1, block(a, f)).wait_send()

            return carry

        lax.fori_loop(0, n_fs, settle, 0)
    last.wait_send()
    last.wait_recv()


def team_layer(
    dims,
    tokens,
    first_gain,
    mixer_gate,
    mixer_value,
    value_gain,
    value_shift,
    spatial_weight,
    spatial_bias,
    mixer_out,
    second_gain,
    up_gate,
    up_value,
    taps_gate,
    taps_value,
    down_proj,
):
    n_rep, n_fs, n_tp = dims
    n_chip, n_line = n_rep * PLANE, n_fs // PLANE
    rows, width = tokens.shape
    half, team_rows = rows // n_tp, rows * n_chip
    cols, hidden_cols = mixer_gate.shape[1] // n_chip, up_gate.shape[1] // n_chip
    vmem, anywhere = pl.BlockSpec(memory_space=pltpu.VMEM), pl.BlockSpec(memory_space=pl.ANY)
    bf16, f32, dma = jnp.bfloat16, jnp.float32, pltpu.SemaphoreType.DMA
    in_specs = [anywhere, vmem, anywhere, anywhere] + [vmem] * 4 + [anywhere, vmem]
    in_specs += [anywhere, anywhere, vmem, vmem, anywhere]
    scratch = [
        pltpu.VMEM((width, cols), bf16),
        pltpu.VMEM((width, cols), bf16),
        pltpu.VMEM((n_fs, mixer_out.shape[0] // n_chip, mixer_out.shape[1]), bf16),
        pltpu.VMEM((width, hidden_cols), bf16),
        pltpu.VMEM((width, hidden_cols), bf16),
        pltpu.VMEM((n_fs, down_proj.shape[0] // n_chip, down_proj.shape[1]), bf16),
        pltpu.VMEM((team_rows, width), bf16),
        pltpu.VMEM((team_rows, width), bf16),
        pltpu.VMEM((team_rows, cols), f32),
        pltpu.VMEM((team_rows, cols), f32),
        pltpu.VMEM((team_rows, cols), bf16),
        pltpu.VMEM((team_rows, hidden_cols), f32),
        pltpu.VMEM((team_rows, hidden_cols), bf16),
        pltpu.VMEM((team_rows, width), bf16),
        pltpu.VMEM((n_chip * half, width), bf16),
        pltpu.VMEM((n_chip - 1, half, width), bf16),
        pltpu.VMEM((half, width), bf16),
        pltpu.VMEM((n_chip * n_tp, 2, team_rows), f32),
        dma((ARRAYS + 1,)),
        dma((ARRAYS, PLANE)),
        dma((ARRAYS, n_fs)),
        dma((ARRAYS, n_fs)),
        dma((ARRAYS, n_fs)),
        dma((2, n_chip)),
        dma((2, n_chip)),
        dma((2, n_chip)),
        dma((2, n_chip)),
        dma((n_chip * n_tp,)),
        dma((n_chip * n_tp,)),
        dma((2, n_line, n_chip)),
        dma((2, n_line, n_chip)),
        dma((2, n_line, 2 * FAR)),
        dma((2, n_line, 2 * FAR)),
        dma((2, n_chip)),
        dma((2, n_chip)),
        dma((2,)),
    ]
    return pl.pallas_call(
        functools.partial(team_kernel, dims),
        out_shape=jax.ShapeDtypeStruct((rows, width), bf16),
        in_specs=in_specs,
        out_specs=vmem,
        scratch_shapes=scratch,
        compiler_params=pltpu.CompilerParams(
            collective_id=0, has_side_effects=True, vmem_limit_bytes=63 * 1024 * 1024
        ),
    )(
        tokens,
        first_gain.reshape(1, -1),
        mixer_gate,
        mixer_value,
        value_gain.reshape(1, -1),
        value_shift.reshape(1, -1),
        spatial_weight,
        spatial_bias,
        mixer_out,
        second_gain.reshape(1, -1),
        up_gate,
        up_value,
        taps_gate,
        taps_value,
        down_proj,
    )


def team_fits(mesh):
    n_rep, n_fs, n_tp = (mesh.shape[name] for name in ("rep", "fs", "tp"))
    if n_tp != 2 or n_rep * PLANE != FAR + 1 or n_fs % PLANE:
        return False
    return D % (n_fs * GDIM) == 0 and D % (n_tp * n_rep * PLANE * GDIM) == 0


def solution(mesh):
    in_specs = (
        P(("rep", "fs"), None),
        P(),
        P("fs", "tp"),
        P("fs", "tp"),
        P(),
        P(),
        P(),
        P(),
        P("tp", "fs"),
        P(),
        P("fs", "tp"),
        P("fs", "tp"),
        P(),
        P(),
        P("tp", "fs"),
    )
    out_specs = P(("rep", "fs"), None)
    body = local
    if team_fits(mesh):
        dims = tuple(mesh.shape[name] for name in ("rep", "fs", "tp"))
        body = functools.partial(team_layer, dims)
    return jax.shard_map(body, mesh=mesh, in_specs=in_specs, out_specs=out_specs, check_vma=False)
```

profile of v0, /device:TPU:0, one launch (start us, length us, event | category | flops | bytes accessed | tf_op | source)
XLA Modules:
  0.0 197.1 jit_solution(1273112630601587246)
XLA Ops:
  0.0 194.3 %shard_map.145 = bf16[384,2048]{1,0:T(8,128)(2,1)} custom-call(bf16[384,2048]{1,0:T(8,128)(2,1)} %tokens.1, f32[1,2048]{1,0:T(1,128)} %bitcast.4, bf16[256,1024]{1,0:T(8,128)(2,1)} %mixer_gate.1, bf16[256,1024]{1,0:T(8,128)(2,1)} %mixer_value.1, f32[1,2048]{1,0:T(1,128)} %bitcast.5, f32[1,2048]{1,0:T(1,128)} %bitcast.6, ...), custom_call_target="tpu_custom_call" | custom-call | tf_op jit(solution)/shard_map/pallas_call | solution.py:748
  194.3 2.7 %copy.17 = bf16[384,2048]{1,0:T(8,128)(2,1)} copy(bf16[384,2048]{1,0:T(8,128)(2,1)} %shard_map.145) | data formatting | bytes 3145728
where the time goes:
time: 197 us
  Pallas kernels  194 us (98%)
  local copies, waits for them, and re-layouts  2.73 us (1%)
    pallas_call x1, Pallas kernels, team_layer(): pl.pallas_call(functools.partial(team_kernel, dims), out_shape=jax.ShapeD...  194 us

commit v1 on v0

--- a/solution.py
+++ b/solution.py
@@ -189,8 +189,8 @@
     rows = tokens.shape[0]
     half = rows // n_tp
     width = tokens.shape[1]
-    sources = (mixer_gate, mixer_value, mixer_out, up_gate, up_value, down_proj)
-    held = (w_gate, w_value, w_out, w_ug, w_uv, w_down)
+    sources = (mixer_value, mixer_gate, mixer_out, up_gate, up_value, down_proj)
+    held = (w_value, w_gate, w_out, w_ug, w_uv, w_down)
     offsets = [(dx, dy) for dx in range(n_rep) for dy in range(n_side)]
     partner = (x, f_own, other)
 
@@ -268,17 +268,26 @@
             return
         for j in range(n_side):
 
-            @pl.when(z - d >= 0)
+            @pl.when((z - d >= 0) & has_up)
             def _():
                 f = (z - d) * n_side + j
                 landed(a, f)
                 send_line(a, f, block(a, f), down=False)
 
-            @pl.when(z + d < n_line)
+            @pl.when((z + d < n_line) & has_down)
             def _():
                 f = (z + d) * n_side + j
                 landed(a, f)
                 send_line(a, f, block(a, f), up=False)
+
+    def arrived(a, d):
+        for j in range(n_side):
+            pl.when((z - d >= 0) & (z == n_line - 1))(lambda: landed(a, (z - d) * n_side + j))
+            pl.when((z + d < n_line) & (z == 0))(lambda: landed(a, (z + d) * n_side + j))
+
+    def arrived_all(a):
+        for d in range(1, n_line):
+            arrived(a, d)
 
     def chip_rows(q, core):
         return pl.ds(pl.multiple_of(q * rows + core * half, half), half)
@@ -345,8 +354,8 @@
     pl.semaphore_wait(barrier, n_chip * n_tp - 1 + neighbours)
 
     my_tokens = tokens.at[pl.ds(pl.multiple_of(c * half, half), half)]
-    for a in range(3):
-        start_side(a)
+    start_side(0)
+    start_side(1)
     start_line(0)
     start_line(1)
     for k in (1, 2):
@@ -355,33 +364,38 @@
         tokens, tok.at[pl.ds(pl.multiple_of(q_own * rows, rows), rows)], own_sem.at[ARRAYS]
     )
     tok_copy.start()
-    for a in range(3, ARRAYS):
-        start_side(a)
+    start_side(2)
     relay(0, 0)
     relay(1, 0)
-    for d in range(1, n_line):
+    relay(0, 1)
+    relay(1, 1)
+    start_line(2)
+    for d in range(2, n_line - 1):
         relay(0, d)
-    start_line(2)
-    relay(2, 0)
     tok_copy.wait()
     norm_chip(q_own)
     for k in (1, 2):
         share_landed(0, k, tok)
         across(0, k, tok).start()
         hand_on(0, k, tok).start()
-    for d in range(1, n_line):
+    relay(2, 0)
+    start_side(3)
+    for d in range(2, n_line - 1):
         relay(1, d)
+    relay(2, 1)
     start_line(3)
-    relay(3, 0)
+    for d in range(2, n_line - 1):
+        relay(2, d)
     for k in (1, 2):
         across_landed(0, k, tok)
     hand_on(0, FAR, tok).start()
-    relay(2, 1)
+    start_side(4)
+    start_side(5)
+    relay(3, 0)
     for k in range(1, n_chip):
         hand_landed(0, k, tok)
         norm_chip(chip_q(k, -1))
-    for d in range(2, n_line - 1):
-        relay(2, d)
+    arrived_all(0)
 
     def project(weight, target):
         tile = half
@@ -425,10 +439,12 @@
 
     for i in range(len(mates)):
         tell(i).start()
+    relay(3, 1)
+    start_line(4)
+    arrived_all(1)
     project(w_gate, gate_act)
-    for d in range(max(2, n_line - 1), n_line):
-        relay(2, d)
-    start_line(4)
+    for d in range(2, n_line - 1):
+        relay(3, d)
     relay(4, 0)
     for i in range(len(mates)):
         tell(i).wait_recv()
@@ -563,12 +579,14 @@
         pass_plane(0, p)
         return carry
 
+    arrived_all(2)
     lax.fori_loop(0, n_line, out_body, 0)
-    relay(3, 1)
+    relay(4, 1)
+    start_line(5)
     lax.fori_loop(0, n_line, pass_body, 0)
-    for d in range(2, n_line):
-        relay(3, d)
-    start_line(5)
+    for d in range(2, n_line - 1):
+        relay(4, d)
+    relay(5, 0)
     lax.fori_loop(0, n_line, functools.partial(finish_plane, 0), 0)
 
     def residual_body(i, carry):
@@ -583,15 +601,14 @@
     for k in (1, 2):
         share(1, k, rows_in, mine).start()
     hand_on(1, 0, rows_in).start()
-    relay(5, 0)
     lax.fori_loop(0, n_line, functools.partial(drain_plane, 0), 0)
-    relay(4, 1)
+    relay(5, 1)
     for k in (1, 2):
         share_landed(1, k, rows_in)
         across(1, k, rows_in).start()
         hand_on(1, k, rows_in).start()
-    for d in range(2, n_line):
-        relay(4, d)
+    for d in range(2, n_line - 1):
+        relay(5, d)
     for k in (1, 2):
         across_landed(1, k, rows_in)
     hand_on(1, FAR, rows_in).start()
@@ -620,8 +637,9 @@
                 gate_half[here, :] = jax.nn.silu(done)
         return carry
 
+    arrived_all(3)
     lax.fori_loop(0, n_chip, functools.partial(raise_body, w_ug, taps_gate, False), 0)
-    relay(5, 1)
+    arrived_all(4)
     lax.fori_loop(0, n_chip, functools.partial(raise_body, w_uv, taps_value, True), 0)
 
     def at_distance(d, act):
@@ -630,8 +648,8 @@
             pl.when(z + d < n_line)(lambda: act(z + d))
 
     for d in range(n_line):
-        if d > 1:
-            relay(5, d)
+        if d:
+            arrived(5, d)
         at_distance(d, lambda p: out_plane(1, p, hidden, w_down))
         if d:
             at_distance(d - 1, lambda p: pass_plane(1, p))

time: 197 us -> 182 us (0.924)
  Pallas kernels: 194 us -> 179 us
    pallas_call x1, Pallas kernels: 194 us -> 179 us  [team_layer(): pl.pallas_call(functools.partial(team_kernel, dims), out_shape=jax.ShapeD...]
where the time goes in v1:
time: 182 us; the launch traced here: 181 us
  Pallas kernels  179 us (98%)
  local copies, waits for them, and re-layouts  2.73 us (2%)
    pallas_call x1, Pallas kernels, team_layer(): pl.pallas_call(functools.partial(team_kernel, dims), out_shape=jax.ShapeD...  179 us

profile of v1, /device:TPU:0, one launch (start us, length us, event | category | flops | bytes accessed | tf_op | source)
XLA Modules:
  0.0 181.3 jit_solution(4317267984888294538)
XLA Ops:
  0.0 178.6 %shard_map.145 = bf16[384,2048]{1,0:T(8,128)(2,1)} custom-call(bf16[384,2048]{1,0:T(8,128)(2,1)} %tokens.1, f32[1,2048]{1,0:T(1,128)} %bitcast.4, bf16[256,1024]{1,0:T(8,128)(2,1)} %mixer_gate.1, bf16[256,1024]{1,0:T(8,128)(2,1)} %mixer_value.1, f32[1,2048]{1,0:T(1,128)} %bitcast.5, f32[1,2048]{1,0:T(1,128)} %bitcast.6, ...), custom_call_target="tpu_custom_call" | custom-call | tf_op jit(solution)/shard_map/pallas_call | solution.py:766
  178.6 2.7 %copy.17 = bf16[384,2048]{1,0:T(8,128)(2,1)} copy(bf16[384,2048]{1,0:T(8,128)(2,1)} %shard_map.145) | data formatting | bytes 3145728

commit v2 on v0

v2 whole, which is shorter than its diff:
```python
import functools

import jax
import jax.numpy as jnp
from jax import lax
from jax.experimental import pallas as pl
from jax.experimental.pallas import tpu as pltpu
from jax.sharding import PartitionSpec as P

D = 2048
GDIM = 128
BLK = 128
LEN = 128


def normalize(matrix, scale_gain):
    values = matrix.astype(jnp.float32)
    factor = lax.rsqrt(jnp.mean(values * values, axis=-1, keepdims=True) + 1e-06)
    return (values * factor * scale_gain).astype(jnp.bfloat16)


def causal_conv(values, tap_weights):
    by_sequence = values.reshape(-1, LEN, values.shape[-1])
    padded = jnp.pad(by_sequence, ((0, 0), (2, 0), (0, 0)))
    summed = (
        tap_weights[0] * padded[:, 0:LEN]
        + tap_weights[1] * padded[:, 1 : LEN + 1]
        + tap_weights[2] * padded[:, 2 : LEN + 2]
    )
    return summed.reshape(values.shape)


def local(
    tokens,
    first_gain,
    mixer_gate,
    mixer_value,
    value_gain,
    value_shift,
    spatial_weight,
    spatial_bias,
    mixer_out,
    second_gain,
    up_gate,
    up_value,
    taps_gate,
    taps_value,
    down_proj,
):
    n_rep, n_tp = lax.axis_size("rep"), lax.axis_size("tp")
    rep_index, tp_index = lax.axis_index("rep"), lax.axis_index("tp")
    team = ("rep", "tp")

    def part(array, axis):
        width = array.shape[axis] // n_rep
        return lax.dynamic_slice_in_dim(array, rep_index * width, width, axis)

    def own(array, width, axis):
        at = (tp_index * n_rep + rep_index) * width
        return lax.dynamic_slice_in_dim(array, at, width, axis)

    w_gate = lax.all_gather(part(mixer_gate, 1), "fs", axis=0, tiled=True)
    w_value = lax.all_gather(part(mixer_value, 1), "fs", axis=0, tiled=True)
    w_out = lax.all_gather(part(mixer_out, 0), "fs", axis=1, tiled=True)
    u_gate = lax.all_gather(part(up_gate, 1), "fs", axis=0, tiled=True)
    u_value = lax.all_gather(part(up_value, 1), "fs", axis=0, tiled=True)
    w_down = lax.all_gather(part(down_proj, 0), "fs", axis=1, tiled=True)

    row_share = tokens.shape[0] // n_tp
    kept_tokens = lax.dynamic_slice_in_dim(tokens, tp_index * row_share, row_share, 0)
    first = lax.all_gather(normalize(kept_tokens, first_gain), team, axis=0, tiled=True)
    row_count = first.shape[0]
    cols = w_gate.shape[1]
    gate_act = jax.nn.gelu(jnp.dot(first, w_gate, preferred_element_type=jnp.float32))
    value_act = jax.nn.gelu(jnp.dot(first, w_value, preferred_element_type=jnp.float32))
    value_sum, value_squares = lax.psum(
        (jnp.sum(value_act, axis=1), jnp.sum(value_act * value_act, axis=1)), team
    )
    row_mean = value_sum / D
    variance = value_squares / D - row_mean * row_mean
    centred = (
        (value_act - row_mean[:, None])
        * lax.rsqrt(variance[:, None] + 1e-05)
        * own(value_gain, cols, 0)
        + own(value_shift, cols, 0)
    ).astype(jnp.bfloat16)
    groups = cols // GDIM
    masked = own(spatial_weight, groups, 0) * jnp.tril(jnp.ones((BLK, BLK), jnp.bfloat16))
    blocks = centred.reshape(row_count // BLK, BLK, groups, GDIM)
    mixed_rows = (
        jnp.einsum("gts,bsgc->btgc", masked, blocks, preferred_element_type=jnp.float32)
        + own(spatial_bias, groups, 0).T[None, :, :, None]
    )
    gated_rows = (gate_act * mixed_rows.reshape(row_count, cols)).astype(jnp.bfloat16)
    summed = lax.psum_scatter(
        jnp.dot(gated_rows, w_out, preferred_element_type=jnp.float32).astype(jnp.bfloat16),
        team,
        scatter_dimension=0,
        tiled=True,
    ).astype(jnp.float32)
    residual = (kept_tokens.astype(jnp.float32) + summed).astype(jnp.bfloat16)
    second = lax.all_gather(normalize(residual, second_gain), team, axis=0, tiled=True)
    hidden_cols = u_gate.shape[1]
    gate_up = jnp.dot(second, u_gate, preferred_element_type=jnp.float32)
    value_up = jnp.dot(second, u_value, preferred_element_type=jnp.float32)
    hidden = (
        jax.nn.silu(causal_conv(gate_up, own(taps_gate, hidden_cols, 1)))
        * causal_conv(value_up, own(taps_value, hidden_cols, 1))
    ).astype(jnp.bfloat16)
    ffn_total = lax.psum_scatter(
        jnp.dot(hidden, w_down, preferred_element_type=jnp.float32).astype(jnp.bfloat16),
        team,
        scatter_dimension=0,
        tiled=True,
    ).astype(jnp.float32)
    final_rows = (residual.astype(jnp.float32) + ffn_total).astype(jnp.bfloat16)
    return lax.all_gather(final_rows, "tp", axis=0, tiled=True)


PLANE = 2
ARRAYS = 6
FAR = 3
MESH = pl.DeviceIdType.MESH


def team_kernel(
    dims,
    tokens,
    first_gain,
    mixer_gate,
    mixer_value,
    value_gain,
    value_shift,
    spatial_weight,
    spatial_bias,
    mixer_out,
    second_gain,
    up_gate,
    up_value,
    taps_gate,
    taps_value,
    down_proj,
    out,
    w_gate,
    w_value,
    w_out,
    w_ug,
    w_uv,
    w_down,
    tok,
    rows_in,
    gate_act,
    value_act,
    gated,
    gate_half,
    hidden,
    part,
    from_partner,
    from_team,
    residual,
    stats,
    mixing,
    taps,
    own_sem,
    side_send,
    up_send,
    down_send,
    weight_recv,
    team_send,
    team_recv,
    pass_send,
    pass_recv,
    stat_sem,
    pair_send,
    pair_recv,
    sum_send,
    sum_recv,
    cross_send,
    cross_recv,
    last_sem,
    local_sem,
):
    n_rep, n_fs, n_tp = dims
    n_side, n_line = PLANE, n_fs // PLANE
    n_chip = n_rep * n_side
    x, c = lax.axis_index("rep"), lax.axis_index("tp")
    f_own = lax.axis_index("fs")
    z, y = f_own // n_side, f_own % n_side
    other = (c + 1) % n_tp
    q_own = x * n_side + y
    rows = tokens.shape[0]
    half = rows // n_tp
    width = tokens.shape[1]
    sources = (mixer_value, mixer_gate, mixer_out, up_gate, up_value, down_proj)
    held = (w_value, w_gate, w_out, w_ug, w_uv, w_down)
    partner = (x, f_own, other)
    has_up, has_down = z + 1 < n_line, z >= 1
    at_end = (z == 0) | (z == n_line - 1)

    def chip_to(k, core):
        dx, dy = k // n_side, k % n_side
        return ((x + dx) % n_rep, z * n_side + (y + dy) % n_side, core)

    def chip_q(k, sign):
        dx, dy = k // n_side, k % n_side
        return ((x + sign * dx + n_rep) % n_rep) * n_side + (y + sign * dy + n_side) % n_side

    def remote(src, dst, send, recv, device):
        return pltpu.make_async_remote_copy(
            src_ref=src, dst_ref=dst, send_sem=send, recv_sem=recv, device_id=device, device_id_type=MESH
        )

    def all_sent(ref, sem):
        remote(ref, ref, sem, sem, partner).wait_send()

    def blocks_of(a, f, count):
        if len(held[a].shape) == 3:
            return held[a].at[pl.ds(f, count)]
        height = sources[a].shape[0]
        return held[a].at[pl.ds(pl.multiple_of(f * height, height), count * height)]

    def block(a, f):
        return held[a].at[f] if len(held[a].shape) == 3 else blocks_of(a, f, 1)

    def piece(a, q):
        if len(held[a].shape) == 3:
            height = sources[a].shape[0] // n_chip
            return sources[a].at[pl.ds(pl.multiple_of(q * height, height), height)]
        cols = sources[a].shape[1] // n_chip
        return sources[a].at[:, pl.ds(pl.multiple_of(q * cols, cols), cols)]

    def own_copy(a):
        return pltpu.make_async_copy(piece(a, q_own), block(a, f_own), own_sem.at[a])

    def side(a):
        to_y = (y + 1) % n_side
        return remote(
            piece(a, x * n_side + to_y),
            block(a, f_own),
            side_send.at[a],
            weight_recv.at[a, f_own],
            (x, z * n_side + to_y, c),
        )

    def along(a, f, step, src):
        sem = up_send if step == 1 else down_send
        return remote(
            src, block(a, f), sem.at[a], weight_recv.at[a, f], (x, f_own + step * n_side, c)
        )

    def landed(a, f):
        remote(block(a, f), block(a, f), side_send.at[a], weight_recv.at[a, f], partner).wait_recv()

    def send_line(a, f, src, up=True, down=True):
        if up:
            pl.when(has_up)(lambda: along(a, f, 1, src).start())
        if down:
            pl.when(has_down)(lambda: along(a, f, -1, src).start())

    def start_side(a):
        own_copy(a).start()
        side(a).start()

    def start_line(a):
        send_line(a, f_own, piece(a, q_own))

    def relay(a, *distances):
        for d in distances:
            if d == 0:
                f = z * n_side + (y + 1) % n_side
                landed(a, f)
                send_line(a, f, block(a, f))
                own_copy(a).wait()
                continue
            for j in range(n_side):

                @pl.when((z - d >= 0) & has_up)
                def _():
                    f = (z - d) * n_side + j
                    landed(a, f)
                    send_line(a, f, block(a, f), down=False)

                @pl.when((z + d < n_line) & has_down)
                def _():
                    f = (z + d) * n_side + j
                    landed(a, f)
                    send_line(a, f, block(a, f), up=False)

    beyond = tuple(range(2, n_line - 1))

    def arrived(a, f):
        pl.when(at_end & (f // n_side != z))(lambda: landed(a, f))

    def arrived_all(a):
        def body(f, carry):
            arrived(a, f)
            return carry

        lax.fori_loop(0, n_fs, body, 0)

    def chip_rows(q, core):
        return pl.ds(pl.multiple_of(q * rows + core * half, half), half)

    cuts = (half * 2 // 3 // 16 * 16, half // 2 // 16 * 16)

    def strip(g, k, forwarded):
        low = (k == 1) == forwarded
        return (0, cuts[g]) if low else (cuts[g], half - cuts[g])

    def strip_rows(buffer, g, k, forwarded, q):
        first, size = strip(g, k, forwarded)
        at = pl.multiple_of(q * rows + c * half + first, 16)
        return buffer.at[pl.ds(at, size)]

    def share(g, k, h, buffer, source, base):
        first, size = strip(g, k, h == 0)
        return remote(
            source.at[pl.ds(pl.multiple_of(base + first, 16), size)],
            strip_rows(buffer, g, k, h == 0, q_own),
            team_send.at[g],
            team_recv.at[g, 2 * (k - 1) + h],
            chip_to(k, c),
        )

    def share_landed(g, k, h, buffer):
        place = strip_rows(buffer, g, k, h == 0, chip_q(k, -1))
        sem = team_recv.at[g, 2 * (k - 1) + h]
        remote(place, place, team_send.at[g], sem, partner).wait_recv()

    def across(g, k, buffer):
        place = strip_rows(buffer, g, k, True, chip_q(k, -1))
        return remote(
            place, place, cross_send.at[g], cross_recv.at[g, k - 1], chip_to(FAR - k, c)
        )

    def across_landed(g, k, buffer):
        place = strip_rows(buffer, g, k, True, chip_q(FAR, -1))
        remote(place, place, cross_send.at[g], cross_recv.at[g, k - 1], partner).wait_recv()

    def hand_on(g, k, buffer):
        place = buffer.at[chip_rows(chip_q(k, -1), c)]
        return remote(place, place, pass_send.at[g], pass_recv.at[g, k], partner)

    def hand_landed(g, k, buffer):
        place = buffer.at[chip_rows(chip_q(k, -1), other)]
        remote(place, place, pass_send.at[g], pass_recv.at[g, k], partner).wait_recv()

    def norm_rows(values, gain):
        factor = lax.rsqrt(jnp.mean(values * values, axis=-1, keepdims=True) + 1e-06)
        return (values * factor * gain).astype(jnp.bfloat16)

    step_rows = 64

    def norm_chip(q):
        def body(i, carry):
            at = pl.ds(pl.multiple_of(q * rows + i * step_rows, step_rows), step_rows)
            rows_in[at, :] = norm_rows(tok[at, :].astype(jnp.float32), first_gain[...])
            return carry

        lax.fori_loop(0, rows // step_rows, body, 0)

    cols, hidden_cols = w_gate.shape[1], w_ug.shape[1]
    groups = cols // GDIM
    slot = c * n_chip + q_own
    at_hidden = pl.ds(pl.multiple_of(slot * hidden_cols, hidden_cols), hidden_cols)
    locals_in = (
        pltpu.make_async_copy(
            spatial_weight.at[pl.ds(slot * groups, groups)], mixing, local_sem.at[0]
        ),
        pltpu.make_async_copy(taps_gate.at[:, at_hidden], taps.at[0], local_sem.at[1]),
        pltpu.make_async_copy(taps_value.at[:, at_hidden], taps.at[1], local_sem.at[2]),
    )

    barrier = pltpu.get_barrier_semaphore()
    for k in range(n_chip):
        for core in (c, other):
            if k or core is other:
                pl.semaphore_signal(barrier, inc=1, device_id=chip_to(k, core), device_id_type=MESH)
    for flag, step in ((has_up, 1), (has_down, -1)):

        @pl.when(flag)
        def _():
            pl.semaphore_signal(
                barrier, inc=1, device_id=(x, f_own + step * n_side, c), device_id_type=MESH
            )

    neighbours = has_up.astype(jnp.int32) + has_down.astype(jnp.int32)
    pl.semaphore_wait(barrier, n_chip * n_tp - 1 + neighbours)

    for a in (0, 1):
        start_side(a)
        start_line(a)
    for h in (0, 1):
        for k in (2, 1):
            share(0, k, h, tok, tokens, c * half).start()
    tok_copy = pltpu.make_async_copy(
        tokens, tok.at[pl.ds(pl.multiple_of(q_own * rows, rows), rows)], own_sem.at[ARRAYS]
    )
    tok_copy.start()
    start_side(2)
    for copy in locals_in:
        copy.start()
    relay(0, 0)
    relay(1, 0)
    relay(0, 1)
    tok_copy.wait()
    norm_chip(q_own)
    share_landed(0, 2, 0, tok)
    across(0, 2, tok).start()
    relay(1, 1)
    share_landed(0, 1, 0, tok)
    across(0, 1, tok).start()
    start_side(3)
    relay(0, *beyond)
    share_landed(0, 2, 1, tok)
    hand_on(0, 2, tok).start()
    hand_landed(0, 2, tok)
    norm_chip(chip_q(2, -1))
    relay(1, *beyond)
    start_line(2)
    share_landed(0, 1, 1, tok)
    hand_on(0, 1, tok).start()
    relay(2, 0)
    hand_landed(0, 1, tok)
    norm_chip(chip_q(1, -1))
    relay(2, 1)
    for k in (1, 2):
        across_landed(0, k, tok)
    hand_on(0, FAR, tok).start()
    hand_landed(0, FAR, tok)
    norm_chip(chip_q(FAR, -1))

    def project(weight, target):
        def body(i, carry):
            at = pl.ds(pl.multiple_of(i * half, half), half)
            product = jnp.dot(rows_in[at, :], weight[...], preferred_element_type=jnp.float32)
            target[at, :] = jax.nn.gelu(product)
            return carry

        lax.fori_loop(0, n_chip * n_tp, body, 0)

    blocks = n_chip * rows // BLK
    lane = lax.broadcasted_iota(jnp.int32, (BLK, BLK), 1)
    sub = lax.broadcasted_iota(jnp.int32, (BLK, BLK), 0)
    arrived_all(0)
    project(w_value, value_act)

    def stat_body(i, carry):
        at = pl.ds(pl.multiple_of(i * BLK, BLK), BLK)
        values = value_act[at, :]
        total = jnp.sum(values, axis=1, keepdims=True)
        squares = jnp.sum(values * values, axis=1, keepdims=True)
        both = jnp.where(lane == 0, total, squares).T
        stats[0, :, at] = both[0:2, :]
        return carry

    lax.fori_loop(0, blocks, stat_body, 0)
    mates = [(k, j) for k in range(n_chip) for j in range(n_tp) if k or j]

    def tell(i):
        k, j = mates[i]
        device = chip_to(k, (c + j) % n_tp)
        return remote(stats.at[0], stats.at[i + 1], stat_sem.at[0], stat_sem.at[1], device)

    for i in range(len(mates)):
        tell(i).start()
    start_side(4)
    relay(2, *beyond)
    start_line(3)
    arrived_all(1)
    project(w_gate, gate_act)
    relay(3, 0)
    told = stats.at[pl.ds(1, len(mates))]
    remote(told, told, stat_sem.at[0], stat_sem.at[1], partner).wait_recv()
    for copy in locals_in:
        copy.wait()
    at_cols = pl.ds(pl.multiple_of(slot * cols, cols), cols)

    def mix_body(i, carry):
        at = pl.ds(pl.multiple_of(i * BLK, BLK), BLK)
        total = stats[0, :, at]
        for s in range(1, len(mates) + 1):
            total = total + stats[s, :, at]
        row_mean = jnp.broadcast_to(total[0:1, :] / width, (BLK, BLK)).T[:, 0:1]
        row_square = jnp.broadcast_to(total[1:2, :] / width, (BLK, BLK)).T[:, 0:1]
        variance = row_square - row_mean * row_mean
        centred = (
            (value_act[at, :] - row_mean) * lax.rsqrt(variance + 1e-05) * value_gain[:, at_cols]
            + value_shift[:, at_cols]
        ).astype(jnp.bfloat16)
        for g in range(groups):
            group = slot * groups + g
            matrix = mixing[g]
            matrix = jnp.where(sub >= lane, matrix, jnp.zeros_like(matrix))
            bias = jnp.broadcast_to(spatial_bias[pl.ds(group, 1), :], (BLK, BLK)).T
            mixed = (
                jnp.dot(
                    matrix, centred[:, g * GDIM : (g + 1) * GDIM], preferred_element_type=jnp.float32
                )
                + bias
            )
            channels = slice(g * GDIM, (g + 1) * GDIM)
            gated[at, channels] = (gate_act[at, channels] * mixed).astype(jnp.bfloat16)
        return carry

    lax.fori_loop(0, blocks, mix_body, 0)

    cut = w_out.shape[2]

    low = z < n_line // 2
    near_z = jnp.where(low, z, n_line - 1 - z)

    def line_f(u):
        i = u // n_side
        turn = near_z - (i + 1) // 2 if i % 2 else near_z + i // 2
        p = jnp.where(i > 2 * near_z, i, turn)
        return jnp.where(low, p, n_line - 1 - p) * n_side + u % n_side

    def unit_cols(u):
        return pl.ds(pl.multiple_of(line_f(u) * cut, cut), cut)

    def pair(u, i):
        q, place = chip_q(FAR - i, 1), unit_cols(u)
        return remote(
            part.at[chip_rows(q, other), place],
            from_partner.at[pl.ds(pl.multiple_of(q * half, half), half), place],
            pair_send.at[0],
            pair_recv.at[u, jnp.minimum(i, 1)],
            partner,
        )

    def lane_cols(u, near):
        return pl.ds(pl.multiple_of(line_f(u) * cut + (2 - near) * (cut // 2), cut // 2), cut // 2)

    def to_team(u, near, t):
        place = lane_cols(u, near)
        k_rows = (near, FAR, FAR - near)[t]
        k_chip = (near, near, FAR - near)[t]
        return remote(
            part.at[chip_rows(chip_q(k_rows, 1), c), place],
            from_team.at[t, :, place],
            sum_send.at[0],
            sum_recv.at[u, t % 2],
            chip_to(k_chip, c),
        )

    def multiply(u, acts, weight):
        def body(i, carry):
            q = chip_q(FAR - i, 1)
            at = pl.ds(pl.multiple_of(q * rows, rows), rows)
            part[at, unit_cols(u)] = jnp.dot(
                acts[at, :], weight[line_f(u)], preferred_element_type=jnp.float32
            ).astype(jnp.bfloat16)
            pair(u, i).start()
            return carry

        lax.fori_loop(0, n_chip, body, 0)

    def pair_landed(u, i):
        whole = from_partner.at[pl.ds(0, (1 + i * (n_chip - 2)) * half), unit_cols(u)]
        remote(whole, whole, pair_send.at[0], pair_recv.at[u, i], partner).wait_recv()

    def reduce_pair(u):
        place = unit_cols(u)
        for k in range(FAR, -1, -1):
            if k >= FAR - 1:
                pair_landed(u, FAR - k)
            q = chip_q(k, 1)
            at = chip_rows(q, c)
            part[at, place] = (
                part[at, place].astype(jnp.float32)
                + from_partner[pl.ds(pl.multiple_of(q * half, half), half), place].astype(
                    jnp.float32
                )
            ).astype(jnp.bfloat16)
            if k == FAR:
                for near in (2, 1):
                    to_team(u, near, 1).start()
            elif k:
                to_team(u, k, 0).start()

    def pass_on(u):
        both = from_team.at[1, :, unit_cols(u)]
        remote(both, both, sum_send.at[0], sum_recv.at[u, 1], partner).wait_recv()
        for near in (2, 1):
            at, place = chip_rows(chip_q(FAR - near, 1), c), lane_cols(u, near)
            part[at, place] = (
                part[at, place].astype(jnp.float32) + from_team[1, :, place].astype(jnp.float32)
            ).astype(jnp.bfloat16)
            to_team(u, near, 2).start()

    def collected(u):
        rest = from_team.at[pl.ds(0, 2), :, unit_cols(u)]
        remote(rest, rest, sum_send.at[0], sum_recv.at[u, 0], partner).wait_recv()

    units = n_line * n_side
    lag = 2

    def out_units(acts, weight, a):
        for u in range(units):
            if u == units // 2:
                relay(3, 1)
                start_line(4)
            arrived(a, line_f(u))
            multiply(u, acts, weight)
            if u:
                reduce_pair(u - 1)
            if u >= 2 * lag:
                pass_on(u - 2 * lag)
        reduce_pair(units - 1)

    out_units(gated, w_out, 2)
    for u in range(units - 2 * lag, units):
        pass_on(u)
    relay(3, *beyond)
    relay(4, 0)
    for u in range(units):
        collected(u)

    def residual_body(i, carry):
        at = pl.ds(pl.multiple_of(i * step_rows, step_rows), step_rows)
        mine = pl.ds(pl.multiple_of(q_own * rows + c * half + i * step_rows, step_rows), step_rows)
        total = part[mine, :].astype(jnp.float32)
        for t in (0, 2):
            total = total + from_team[t, at, :].astype(jnp.float32)
        kept = (tok[mine, :].astype(jnp.float32) + total).astype(jnp.bfloat16)
        residual[at, :] = kept
        rows_in[mine, :] = norm_rows(kept.astype(jnp.float32), second_gain[...])
        return carry

    lax.fori_loop(0, half // step_rows, residual_body, 0)
    for h in (0, 1):
        for k in (1, 2):
            share(1, k, h, rows_in, rows_in, q_own * rows + c * half).start()
    hand_on(1, 0, rows_in).start()
    all_sent(from_partner, pair_send.at[0])
    all_sent(from_team, sum_send.at[0])
    for k in (1, 2):
        share_landed(1, k, 0, rows_in)
        across(1, k, rows_in).start()
    start_side(5)
    relay(4, 1)
    for k in (1, 2):
        share_landed(1, k, 1, rows_in)
        hand_on(1, k, rows_in).start()
    relay(4, *beyond)
    start_line(5)

    position = lax.broadcasted_iota(jnp.int32, (LEN, hidden_cols), 0)

    def conv(values, which):
        back1 = jnp.where(position >= 1, pltpu.roll(values, 1, 0), 0.0)
        back2 = jnp.where(position >= 2, pltpu.roll(values, 2, 0), 0.0)
        weights = taps[which]
        return weights[0:1] * back2 + weights[1:2] * back1 + weights[2:3] * values

    def raise_chip(weight, which, q):
        at = pl.ds(pl.multiple_of(q * rows, rows), rows)
        product = jnp.dot(rows_in[at, :], weight[...], preferred_element_type=jnp.float32)
        for s in range(rows // LEN):
            here = pl.ds(pl.multiple_of(q * rows + s * LEN, LEN), LEN)
            done = conv(product[s * LEN : (s + 1) * LEN], which)
            if which:
                hidden[here, :] = (gate_half[here, :] * done).astype(jnp.bfloat16)
            else:
                gate_half[here, :] = jax.nn.silu(done)

    def raise_gate(k, carry):
        hand_landed(1, k, rows_in)
        raise_chip(w_ug, 0, chip_q(k, -1))
        return carry

    def raise_value(q, carry):
        raise_chip(w_uv, 1, q)
        return carry

    arrived_all(3)
    lax.fori_loop(0, FAR, raise_gate, 0)
    for k in (1, 2):
        across_landed(1, k, rows_in)
    hand_on(1, FAR, rows_in).start()
    relay(5, 0)
    lax.fori_loop(FAR, n_chip, raise_gate, 0)
    arrived_all(4)
    lax.fori_loop(0, n_chip, raise_value, 0)

    def finish(u):
        collected(u)
        place = unit_cols(u)
        mine = chip_rows(q_own, c)
        here = pl.ds(pl.multiple_of(c * half, half), half)
        total = part[mine, place].astype(jnp.float32)
        for t in (0, 2):
            total = total + from_team[t, :, place].astype(jnp.float32)
        out[here, place] = (residual[:, place].astype(jnp.float32) + total).astype(jnp.bfloat16)
        done = out.at[here, place]
        remote(done, done, last_sem.at[0], last_sem.at[1], partner).start()

    passed = 0
    for u in range(units):
        if u == n_side:
            relay(5, 1)
        elif u % n_side == 0 and u // n_side - 1 in beyond:
            relay(5, u // n_side - 1)
        arrived(5, line_f(u))
        multiply(u, hidden, w_down)
        for v in range(passed, u if u > units // 2 else u - 1):
            pass_on(v)
            passed = v + 1
        reduce_pair(u)
    for u in range(units - 2):
        finish(u)
    pass_on(units - 1)
    for u in range(units - 2, units):
        finish(u)

    for a in range(ARRAYS):
        all_sent(block(a, 0), side_send.at[a])
        for n in range(1, n_line):
            pl.when(z == n - 1)(lambda: all_sent(blocks_of(a, 0, n * n_side), up_send.at[a]))
            pl.when(z == n)(
                lambda: all_sent(
                    blocks_of(a, n * n_side, (n_line - n) * n_side), down_send.at[a]
                )
            )
    all_sent(told, stat_sem.at[0])
    for g in range(2):
        all_sent(tok.at[pl.ds(0, rows)], team_send.at[g])
        all_sent(tok.at[pl.ds(0, half)], cross_send.at[g])
        all_sent(tok.at[pl.ds(0, (n_chip - 1 + g) * half)], pass_send.at[g])
    all_sent(from_partner, pair_send.at[0])
    all_sent(from_team, sum_send.at[0])
    theirs = out.at[pl.ds(pl.multiple_of(other * half, half), half)]
    last = remote(theirs, theirs, last_sem.at[0], last_sem.at[1], partner)
    last.wait_send()
    last.wait_recv()


def team_layer(
    dims,
    tokens,
    first_gain,
    mixer_gate,
    mixer_value,
    value_gain,
    value_shift,
    spatial_weight,
    spatial_bias,
    mixer_out,
    second_gain,
    up_gate,
    up_value,
    taps_gate,
    taps_value,
    down_proj,
):
    n_rep, n_fs, n_tp = dims
    n_chip, n_line = n_rep * PLANE, n_fs // PLANE
    rows, width = tokens.shape
    half, team_rows = rows // n_tp, rows * n_chip
    cols, hidden_cols = mixer_gate.shape[1] // n_chip, up_gate.shape[1] // n_chip
    vmem, anywhere = pl.BlockSpec(memory_space=pltpu.VMEM), pl.BlockSpec(memory_space=pl.ANY)
    bf16, f32, dma = jnp.bfloat16, jnp.float32, pltpu.SemaphoreType.DMA
    in_specs = [anywhere, vmem, anywhere, anywhere, vmem, vmem, anywhere, vmem, anywhere, vmem]
    in_specs += [anywhere] * 5
    units = n_fs
    scratch = [
        pltpu.VMEM((width, cols), bf16),
        pltpu.VMEM((width, cols), bf16),
        pltpu.VMEM((n_fs, mixer_out.shape[0] // n_chip, mixer_out.shape[1]), bf16),
        pltpu.VMEM((width, hidden_cols), bf16),
        pltpu.VMEM((width, hidden_cols), bf16),
        pltpu.VMEM((n_fs, down_proj.shape[0] // n_chip, down_proj.shape[1]), bf16),
        pltpu.VMEM((team_rows, width), bf16),
        pltpu.VMEM((team_rows, width), bf16),
        pltpu.VMEM((team_rows, cols), f32),
        pltpu.VMEM((team_rows, cols), f32),
        pltpu.VMEM((team_rows, cols), bf16),
        pltpu.VMEM((team_rows, hidden_cols), f32),
        pltpu.VMEM((team_rows, hidden_cols), bf16),
        pltpu.VMEM((team_rows, width), bf16),
        pltpu.VMEM((n_chip * half, width), bf16),
        pltpu.VMEM((n_chip - 1, half, width), bf16),
        pltpu.VMEM((half, width), bf16),
        pltpu.VMEM((n_chip * n_tp, 2, team_rows), f32),
        pltpu.VMEM((cols // GDIM,) + spatial_weight.shape[1:], bf16),
        pltpu.VMEM((2, 3, hidden_cols), f32),
        dma((ARRAYS + 1,)),
        dma((ARRAYS,)),
        dma((ARRAYS,)),
        dma((ARRAYS,)),
        dma((ARRAYS, n_fs)),
        dma((2,)),
        dma((2, 4)),
        dma((2,)),
        dma((2, n_chip)),
        dma((2,)),
        dma((1,)),
        dma((units, 2)),
        dma((1,)),
        dma((units, 2)),
        dma((2,)),
        dma((2, 2)),
        dma((2,)),
        dma((3,)),
    ]
    return pl.pallas_call(
        functools.partial(team_kernel, dims),
        out_shape=pltpu.VMEM((rows, width), bf16),
        in_specs=in_specs,
        out_specs=vmem,
        scratch_shapes=scratch,
        compiler_params=pltpu.CompilerParams(
            collective_id=0, has_side_effects=True, vmem_limit_bytes=56 * 1024 * 1024
        ),
    )(
        tokens,
        first_gain.reshape(1, -1),
        mixer_gate,
        mixer_value,
        value_gain.reshape(1, -1),
        value_shift.reshape(1, -1),
        spatial_weight,
        spatial_bias,
        mixer_out,
        second_gain.reshape(1, -1),
        up_gate,
        up_value,
        taps_gate,
        taps_value,
        down_proj,
    )


def team_fits(mesh):
    n_rep, n_fs, n_tp = (mesh.shape[name] for name in ("rep", "fs", "tp"))
    if n_tp != 2 or n_rep * PLANE != FAR + 1 or n_fs % PLANE:
        return False
    return D % (n_fs * GDIM) == 0 and D % (n_tp * n_rep * PLANE * GDIM) == 0


def solution(mesh):
    in_specs = (
        P(("rep", "fs"), None),
        P(),
        P("fs", "tp"),
        P("fs", "tp"),
        P(),
        P(),
        P(),
        P(),
        P("tp", "fs"),
        P(),
        P("fs", "tp"),
        P("fs", "tp"),
        P(),
        P(),
        P("tp", "fs"),
    )
    out_specs = P(("rep", "fs"), None)
    body = local
    if team_fits(mesh):
        dims = tuple(mesh.shape[name] for name in ("rep", "fs", "tp"))
        body = functools.partial(team_layer, dims)
    return jax.shard_map(body, mesh=mesh, in_specs=in_specs, out_specs=out_specs, check_vma=False)
```

time: 197 us -> 172 us (0.87)
  Pallas kernels: 194 us -> 170 us
    pallas_call x1, Pallas kernels: 194 us -> 170 us  [team_layer(): pl.pallas_call(functools.partial(team_kernel, dims), out_shape=pltpu.VMEM...]
where the time goes in v2:
time: 172 us; the launch traced here: 171 us
  Pallas kernels  170 us (99%)
    pallas_call x1, Pallas kernels, team_layer(): pl.pallas_call(functools.partial(team_kernel, dims), out_shape=pltpu.VMEM...  170 us

profile of v2, /device:TPU:0, one launch (start us, length us, event | category | flops | bytes accessed | tf_op | source)
XLA Modules:
  0.0 171.3 jit_solution(8449505073739914312)
XLA Ops:
  0.0 170.2 %shard_map.145 = bf16[384,2048]{1,0:T(8,128)(2,1)S(1)} custom-call(bf16[384,2048]{1,0:T(8,128)(2,1)} %tokens.1, f32[1,2048]{1,0:T(1,128)} %bitcast.4, bf16[256,1024]{1,0:T(8,128)(2,1)} %mixer_gate.1, bf16[256,1024]{1,0:T(8,128)(2,1)} %mixer_value.1, f32[1,2048]{1,0:T(1,128)} %bitcast.5, f32[1,2048]{1,0:T(1,128)} %bitcast.6, ...), custom_call_target="tpu_custom_call" | custom-call | tf_op jit(solution)/shard_map/pallas_call | solution.py:807
  170.2 1.1 copy.17

commit v3 on v2

--- a/solution.py
+++ b/solution.py
@@ -161,6 +161,9 @@
     stats,
     mixing,
     taps,
+    gains,
+    scales,
+    biases,
     own_sem,
     side_send,
     up_send,
@@ -196,6 +199,7 @@
     partner = (x, f_own, other)
     has_up, has_down = z + 1 < n_line, z >= 1
     at_end = (z == 0) | (z == n_line - 1)
+    low = z < n_line // 2
 
     def chip_to(k, core):
         dx, dy = k // n_side, k % n_side
@@ -273,18 +277,23 @@
                 own_copy(a).wait()
                 continue
             for j in range(n_side):
-
-                @pl.when((z - d >= 0) & has_up)
-                def _():
-                    f = (z - d) * n_side + j
-                    landed(a, f)
-                    send_line(a, f, block(a, f), down=False)
-
-                @pl.when((z + d < n_line) & has_down)
-                def _():
-                    f = (z + d) * n_side + j
-                    landed(a, f)
-                    send_line(a, f, block(a, f), up=False)
+                turn = j if a in (2, 5) else (y + j) % n_side
+                for first in (True, False):
+                    above = low if first else jnp.logical_not(low)
+
+                    @pl.when((z + d < n_line) & has_down & above)
+                    def _():
+                        f = (z + d) * n_side + turn
+                        landed(a, f)
+                        send_line(a, f, block(a, f), up=False)
+
+                    if first:
+
+                        @pl.when((z - d >= 0) & has_up)
+                        def _():
+                            f = (z - d) * n_side + turn
+                            landed(a, f)
+                            send_line(a, f, block(a, f), down=False)
 
     beyond = tuple(range(2, n_line - 1))
 
@@ -354,7 +363,7 @@
     def norm_chip(q):
         def body(i, carry):
             at = pl.ds(pl.multiple_of(q * rows + i * step_rows, step_rows), step_rows)
-            rows_in[at, :] = norm_rows(tok[at, :].astype(jnp.float32), first_gain[...])
+            rows_in[at, :] = norm_rows(tok[at, :].astype(jnp.float32), gains[0:1, :])
             return carry
 
         lax.fori_loop(0, rows // step_rows, body, 0)
@@ -363,7 +372,13 @@
     groups = cols // GDIM
     slot = c * n_chip + q_own
     at_hidden = pl.ds(pl.multiple_of(slot * hidden_cols, hidden_cols), hidden_cols)
+    at_cols = pl.ds(pl.multiple_of(slot * cols, cols), cols)
+    first_gain_in = pltpu.make_async_copy(first_gain, gains.at[0:1], local_sem.at[3])
     locals_in = (
+        pltpu.make_async_copy(second_gain, gains.at[1:2], local_sem.at[4]),
+        pltpu.make_async_copy(value_gain.at[:, at_cols], scales.at[0:1], local_sem.at[5]),
+        pltpu.make_async_copy(value_shift.at[:, at_cols], scales.at[1:2], local_sem.at[6]),
+        pltpu.make_async_copy(spatial_bias, biases, local_sem.at[7]),
         pltpu.make_async_copy(
             spatial_weight.at[pl.ds(slot * groups, groups)], mixing, local_sem.at[0]
         ),
@@ -372,10 +387,8 @@
     )
 
     barrier = pltpu.get_barrier_semaphore()
-    for k in range(n_chip):
-        for core in (c, other):
-            if k or core is other:
-                pl.semaphore_signal(barrier, inc=1, device_id=chip_to(k, core), device_id_type=MESH)
+    for mate in (chip_to(1, c), chip_to(2, c), partner):
+        pl.semaphore_signal(barrier, inc=1, device_id=mate, device_id_type=MESH)
     for flag, step in ((has_up, 1), (has_down, -1)):
 
         @pl.when(flag)
@@ -385,7 +398,7 @@
             )
 
     neighbours = has_up.astype(jnp.int32) + has_down.astype(jnp.int32)
-    pl.semaphore_wait(barrier, n_chip * n_tp - 1 + neighbours)
+    pl.semaphore_wait(barrier, FAR + neighbours)
 
     for a in (0, 1):
         start_side(a)
@@ -398,12 +411,14 @@
     )
     tok_copy.start()
     start_side(2)
+    first_gain_in.start()
     for copy in locals_in:
         copy.start()
     relay(0, 0)
     relay(1, 0)
     relay(0, 1)
     tok_copy.wait()
+    first_gain_in.wait()
     norm_chip(q_own)
     share_landed(0, 2, 0, tok)
     across(0, 2, tok).start()
@@ -474,7 +489,6 @@
     remote(told, told, stat_sem.at[0], stat_sem.at[1], partner).wait_recv()
     for copy in locals_in:
         copy.wait()
-    at_cols = pl.ds(pl.multiple_of(slot * cols, cols), cols)
 
     def mix_body(i, carry):
         at = pl.ds(pl.multiple_of(i * BLK, BLK), BLK)
@@ -485,14 +499,14 @@
         row_square = jnp.broadcast_to(total[1:2, :] / width, (BLK, BLK)).T[:, 0:1]
         variance = row_square - row_mean * row_mean
         centred = (
-            (value_act[at, :] - row_mean) * lax.rsqrt(variance + 1e-05) * value_gain[:, at_cols]
-            + value_shift[:, at_cols]
+            (value_act[at, :] - row_mean) * lax.rsqrt(variance + 1e-05) * scales[0:1, :]
+            + scales[1:2, :]
         ).astype(jnp.bfloat16)
         for g in range(groups):
             group = slot * groups + g
             matrix = mixing[g]
             matrix = jnp.where(sub >= lane, matrix, jnp.zeros_like(matrix))
-            bias = jnp.broadcast_to(spatial_bias[pl.ds(group, 1), :], (BLK, BLK)).T
+            bias = jnp.broadcast_to(biases[pl.ds(group, 1), :], (BLK, BLK)).T
             mixed = (
                 jnp.dot(
                     matrix, centred[:, g * GDIM : (g + 1) * GDIM], preferred_element_type=jnp.float32
@@ -506,8 +520,8 @@
     lax.fori_loop(0, blocks, mix_body, 0)
 
     cut = w_out.shape[2]
-
-    low = z < n_line // 2
+    units = n_line * n_side
+
     near_z = jnp.where(low, z, n_line - 1 - z)
 
     def line_f(u):
@@ -593,7 +607,6 @@
         rest = from_team.at[pl.ds(0, 2), :, unit_cols(u)]
         remote(rest, rest, sum_send.at[0], sum_recv.at[u, 0], partner).wait_recv()
 
-    units = n_line * n_side
     lag = 2
 
     def out_units(acts, weight, a):
@@ -625,7 +638,7 @@
             total = total + from_team[t, at, :].astype(jnp.float32)
         kept = (tok[mine, :].astype(jnp.float32) + total).astype(jnp.bfloat16)
         residual[at, :] = kept
-        rows_in[mine, :] = norm_rows(kept.astype(jnp.float32), second_gain[...])
+        rows_in[mine, :] = norm_rows(kept.astype(jnp.float32), gains[1:2, :])
         return carry
 
     lax.fori_loop(0, half // step_rows, residual_body, 0)
@@ -702,17 +715,19 @@
             relay(5, 1)
         elif u % n_side == 0 and u // n_side - 1 in beyond:
             relay(5, u // n_side - 1)
+        early = u > units // 2
+        for v in range(passed, u if early else u - 1):
+            pass_on(v)
+            passed = v + 1
+        if early:
+            finish(u - units // 2 - 1)
         arrived(5, line_f(u))
         multiply(u, hidden, w_down)
-        for v in range(passed, u if u > units // 2 else u - 1):
-            pass_on(v)
-            passed = v + 1
         reduce_pair(u)
-    for u in range(units - 2):
+    for u in range(units - units // 2 - 1, units - 1):
         finish(u)
     pass_on(units - 1)
-    for u in range(units - 2, units):
-        finish(u)
+    finish(units - 1)
 
     for a in range(ARRAYS):
         all_sent(block(a, 0), side_send.at[a])
@@ -761,8 +776,7 @@
     cols, hidden_cols = mixer_gate.shape[1] // n_chip, up_gate.shape[1] // n_chip
     vmem, anywhere = pl.BlockSpec(memory_space=pltpu.VMEM), pl.BlockSpec(memory_space=pl.ANY)
     bf16, f32, dma = jnp.bfloat16, jnp.float32, pltpu.SemaphoreType.DMA
-    in_specs = [anywhere, vmem, anywhere, anywhere, vmem, vmem, anywhere, vmem, anywhere, vmem]
-    in_specs += [anywhere] * 5
+    in_specs = [anywhere] * 15
     units = n_fs
     scratch = [
         pltpu.VMEM((width, cols), bf16),
@@ -785,6 +799,9 @@
         pltpu.VMEM((n_chip * n_tp, 2, team_rows), f32),
         pltpu.VMEM((cols // GDIM,) + spatial_weight.shape[1:], bf16),
         pltpu.VMEM((2, 3, hidden_cols), f32),
+        pltpu.VMEM((2, width), f32),
+        pltpu.VMEM((2, cols), f32),
+        pltpu.VMEM(spatial_bias.shape, f32),
         dma((ARRAYS + 1,)),
         dma((ARRAYS,)),
         dma((ARRAYS,)),
@@ -802,7 +819,7 @@
         dma((2,)),
         dma((2, 2)),
         dma((2,)),
-        dma((3,)),
+        dma((8,)),
     ]
     return pl.pallas_call(
         functools.partial(team_kernel, dims),

time: 172 us -> 169 us (0.983)
  Pallas kernels: 170 us -> 168 us
    pallas_call x1, Pallas kernels: 170 us -> 168 us  [team_layer(): pl.pallas_call(functools.partial(team_kernel, dims), out_shape=pltpu.VMEM...]
where the time goes in v3:
time: 169 us
  Pallas kernels  168 us (99%)
    pallas_call x1, Pallas kernels, team_layer(): pl.pallas_call(functools.partial(team_kernel, dims), out_shape=pltpu.VMEM...  168 us

profile of v3, /device:TPU:0, one launch (start us, length us, event | category | flops | bytes accessed | tf_op | source)
XLA Modules:
  0.0 169.3 jit_solution(7146847072792062864)
XLA Ops:
  0.0 168.1 %shard_map.145 = bf16[384,2048]{1,0:T(8,128)(2,1)S(1)} custom-call(bf16[384,2048]{1,0:T(8,128)(2,1)} %tokens.1, f32[1,2048]{1,0:T(1,128)} %bitcast.4, bf16[256,1024]{1,0:T(8,128)(2,1)} %mixer_gate.1, bf16[256,1024]{1,0:T(8,128)(2,1)} %mixer_value.1, f32[1,2048]{1,0:T(1,128)} %bitcast.5, f32[1,2048]{1,0:T(1,128)} %bitcast.6, ...), custom_call_target="tpu_custom_call" | custom-call | tf_op jit(solution)/shard_map/pallas_call | solution.py:824
  168.2 1.1 copy.17

commit v4 on v3

--- a/solution.py
+++ b/solution.py
@@ -164,6 +164,7 @@
     gains,
     scales,
     biases,
+    ahead,
     own_sem,
     side_send,
     up_send,
@@ -236,10 +237,15 @@
     def own_copy(a):
         return pltpu.make_async_copy(piece(a, q_own), block(a, f_own), own_sem.at[a])
 
+    q_side = x * n_side + (y + 1) % n_side
+
+    def staged(a):
+        return pltpu.make_async_copy(piece(a, q_side), ahead.at[a], local_sem.at[8 + a])
+
     def side(a):
         to_y = (y + 1) % n_side
         return remote(
-            piece(a, x * n_side + to_y),
+            piece(a, q_side) if a > 1 else ahead.at[a],
             block(a, f_own),
             side_send.at[a],
             weight_recv.at[a, f_own],
@@ -274,7 +280,8 @@
                 f = z * n_side + (y + 1) % n_side
                 landed(a, f)
                 send_line(a, f, block(a, f))
-                own_copy(a).wait()
+                if a > 1:
+                    own_copy(a).wait()
                 continue
             for j in range(n_side):
                 turn = j if a in (2, 5) else (y + j) % n_side
@@ -386,6 +393,10 @@
         pltpu.make_async_copy(taps_value.at[:, at_hidden], taps.at[1], local_sem.at[2]),
     )
 
+    for a in (0, 1):
+        own_copy(a).start()
+        staged(a).start()
+
     barrier = pltpu.get_barrier_semaphore()
     for mate in (chip_to(1, c), chip_to(2, c), partner):
         pl.semaphore_signal(barrier, inc=1, device_id=mate, device_id_type=MESH)
@@ -401,8 +412,10 @@
     pl.semaphore_wait(barrier, FAR + neighbours)
 
     for a in (0, 1):
-        start_side(a)
-        start_line(a)
+        own_copy(a).wait()
+        send_line(a, f_own, block(a, f_own))
+        staged(a).wait()
+        side(a).start()
     for h in (0, 1):
         for k in (2, 1):
             share(0, k, h, tok, tokens, c * half).start()
@@ -559,24 +572,27 @@
         )
 
     def multiply(u, acts, weight):
+        band = n_side * rows
+
         def body(i, carry):
-            q = chip_q(FAR - i, 1)
-            at = pl.ds(pl.multiple_of(q * rows, rows), rows)
+            at_x = (x + 1 + i) % n_rep
+            at = pl.ds(pl.multiple_of(at_x * band, band), band)
             part[at, unit_cols(u)] = jnp.dot(
                 acts[at, :], weight[line_f(u)], preferred_element_type=jnp.float32
             ).astype(jnp.bfloat16)
-            pair(u, i).start()
+            for j in range(n_side):
+                pair(u, i * n_side + j).start()
             return carry
 
-        lax.fori_loop(0, n_chip, body, 0)
+        lax.fori_loop(0, n_rep, body, 0)
 
     def pair_landed(u, i):
         whole = from_partner.at[pl.ds(0, (1 + i * (n_chip - 2)) * half), unit_cols(u)]
         remote(whole, whole, pair_send.at[0], pair_recv.at[u, i], partner).wait_recv()
 
-    def reduce_pair(u):
+    def reduce_pair(u, chips=tuple(range(FAR, -1, -1))):
         place = unit_cols(u)
-        for k in range(FAR, -1, -1):
+        for k in chips:
             if k >= FAR - 1:
                 pair_landed(u, FAR - k)
             q = chip_q(k, 1)
@@ -715,18 +731,19 @@
             relay(5, 1)
         elif u % n_side == 0 and u // n_side - 1 in beyond:
             relay(5, u // n_side - 1)
-        early = u > units // 2
-        for v in range(passed, u if early else u - 1):
+        arrived(5, line_f(u))
+        multiply(u, hidden, w_down)
+        reduce_pair(u, (FAR,))
+        for v in range(passed, u if u > units // 2 else u - 1):
             pass_on(v)
             passed = v + 1
-        if early:
+        reduce_pair(u, tuple(range(FAR - 1, -1, -1)))
+        if u > units // 2:
             finish(u - units // 2 - 1)
-        arrived(5, line_f(u))
-        multiply(u, hidden, w_down)
-        reduce_pair(u)
-    for u in range(units - units // 2 - 1, units - 1):
+    for u in range(units - units // 2 - 1, units - 2):
         finish(u)
     pass_on(units - 1)
+    finish(units - 2)
     finish(units - 1)
 
     for a in range(ARRAYS):
@@ -802,6 +819,7 @@
         pltpu.VMEM((2, width), f32),
         pltpu.VMEM((2, cols), f32),
         pltpu.VMEM(spatial_bias.shape, f32),
+        pltpu.VMEM((2, mixer_value.shape[0], cols), bf16),
         dma((ARRAYS + 1,)),
         dma((ARRAYS,)),
         dma((ARRAYS,)),
@@ -819,7 +837,7 @@
         dma((2,)),
         dma((2, 2)),
         dma((2,)),
-        dma((8,)),
+        dma((10,)),
     ]
     return pl.pallas_call(
         functools.partial(team_kernel, dims),

time: 169 us -> 169 us (level)
  no operation moved by 1% of the time
where the time goes in v4:
time: 169 us
  Pallas kernels  168 us (99%)
    pallas_call x1, Pallas kernels, team_layer(): pl.pallas_call(functools.partial(team_kernel, dims), out_shape=pltpu.VMEM...  168 us

profile of v4, /device:TPU:0, one launch (start us, length us, event | category | flops | bytes accessed | tf_op | source)
XLA Modules:
  0.0 168.9 jit_solution(7236378996366667580)
XLA Ops:
  0.0 167.7 %shard_map.145 = bf16[384,2048]{1,0:T(8,128)(2,1)S(1)} custom-call(bf16[384,2048]{1,0:T(8,128)(2,1)} %tokens.1, f32[1,2048]{1,0:T(1,128)} %bitcast.4, bf16[256,1024]{1,0:T(8,128)(2,1)} %mixer_gate.1, bf16[256,1024]{1,0:T(8,128)(2,1)} %mixer_value.1, f32[1,2048]{1,0:T(1,128)} %bitcast.5, f32[1,2048]{1,0:T(1,128)} %bitcast.6, ...), custom_call_target="tpu_custom_call" | custom-call | tf_op jit(solution)/shard_map/pallas_call | solution.py:842
  167.7 1.1 copy.17

commit v5 on v4

--- a/solution.py
+++ b/solution.py
@@ -183,6 +183,7 @@
     cross_recv,
     last_sem,
     local_sem,
+    late_recv,
 ):
     n_rep, n_fs, n_tp = dims
     n_side, n_line = PLANE, n_fs // PLANE
@@ -258,6 +259,21 @@
             src, block(a, f), sem.at[a], weight_recv.at[a, f], (x, f_own + step * n_side, c)
         )
 
+    def halves(a, f):
+        cut = sources[a].shape[1] // 2
+        return [held[a].at[f, :, pl.ds(h * cut, cut)] for h in (0, 1)]
+
+    def send_halves(a, f, step):
+        for h, ref in enumerate(halves(a, f)):
+            sem = up_send if step == 1 else down_send
+            recv = late_recv.at[0] if h else weight_recv.at[a, f]
+            remote(ref, ref, sem.at[a], recv, (x, f_own + step * n_side, c)).start()
+
+    def half_landed(a, f, h):
+        ref = halves(a, f)[h]
+        recv = late_recv.at[0] if h else weight_recv.at[a, f]
+        pl.when(at_end)(lambda: remote(ref, ref, side_send.at[a], recv, partner).wait_recv())
+
     def landed(a, f):
         remote(block(a, f), block(a, f), side_send.at[a], weight_recv.at[a, f], partner).wait_recv()
 
@@ -285,6 +301,7 @@
                 continue
             for j in range(n_side):
                 turn = j if a in (2, 5) else (y + j) % n_side
+                final = a == ARRAYS - 1 and d == n_line - 2 and j == n_side - 1
                 for first in (True, False):
                     above = low if first else jnp.logical_not(low)
 
@@ -292,7 +309,10 @@
                     def _():
                         f = (z + d) * n_side + turn
                         landed(a, f)
-                        send_line(a, f, block(a, f), up=False)
+                        if final:
+                            send_halves(a, f, -1)
+                        else:
+                            send_line(a, f, block(a, f), up=False)
 
                     if first:
 
@@ -300,7 +320,10 @@
                         def _():
                             f = (z - d) * n_side + turn
                             landed(a, f)
-                            send_line(a, f, block(a, f), down=False)
+                            if final:
+                                send_halves(a, f, 1)
+                            else:
+                                send_line(a, f, block(a, f), down=False)
 
     beyond = tuple(range(2, n_line - 1))
 
@@ -543,8 +566,18 @@
         p = jnp.where(i > 2 * near_z, i, turn)
         return jnp.where(low, p, n_line - 1 - p) * n_side + u % n_side
 
+    def shape_of(u):
+        line, low_col, size = min(u, units - 1), 0, cut
+        if isinstance(u, float):
+            line, low_col, size = units - 1, int(u * 2) % 2 * (cut // 2), cut // 2
+        return line, low_col, size
+
+    def sem_of(u):
+        return units - 1 + int(u * 2) % 2 if isinstance(u, float) else u
+
     def unit_cols(u):
-        return pl.ds(pl.multiple_of(line_f(u) * cut, cut), cut)
+        line, low_col, size = shape_of(u)
+        return pl.ds(pl.multiple_of(line_f(line) * cut + low_col, size), size)
 
     def pair(u, i):
         q, place = chip_q(FAR - i, 1), unit_cols(u)
@@ -552,33 +585,45 @@
             part.at[chip_rows(q, other), place],
             from_partner.at[pl.ds(pl.multiple_of(q * half, half), half), place],
             pair_send.at[0],
-            pair_recv.at[u, jnp.minimum(i, 1)],
+            pair_recv.at[sem_of(u), jnp.minimum(i, 1)],
             partner,
         )
 
-    def lane_cols(u, near):
-        return pl.ds(pl.multiple_of(line_f(u) * cut + (2 - near) * (cut // 2), cut // 2), cut // 2)
+    def lane(u, near):
+        line, low_col, size = shape_of(u)
+        if size < cut:
+            return (2 - near) * (half // 2), half // 2, unit_cols(u)
+        size = cut // 2
+        at = line_f(line) * cut + (2 - near) * size
+        return 0, half, pl.ds(pl.multiple_of(at, size), size)
+
+    def lane_part(u, near, q):
+        first, count, place = lane(u, near)
+        return pl.ds(pl.multiple_of(q * rows + c * half + first, 16), count), place
 
     def to_team(u, near, t):
-        place = lane_cols(u, near)
+        first, count, place = lane(u, near)
         k_rows = (near, FAR, FAR - near)[t]
         k_chip = (near, near, FAR - near)[t]
         return remote(
-            part.at[chip_rows(chip_q(k_rows, 1), c), place],
-            from_team.at[t, :, place],
+            part.at[lane_part(u, near, chip_q(k_rows, 1))],
+            from_team.at[t, pl.ds(first, count), place],
             sum_send.at[0],
-            sum_recv.at[u, t % 2],
+            sum_recv.at[sem_of(u), t % 2],
             chip_to(k_chip, c),
         )
 
     def multiply(u, acts, weight):
+        line, low_col, size = shape_of(u)
         band = n_side * rows
 
         def body(i, carry):
             at_x = (x + 1 + i) % n_rep
             at = pl.ds(pl.multiple_of(at_x * band, band), band)
             part[at, unit_cols(u)] = jnp.dot(
-                acts[at, :], weight[line_f(u)], preferred_element_type=jnp.float32
+                acts[at, :],
+                weight[line_f(line), :, low_col : low_col + size],
+                preferred_element_type=jnp.float32,
             ).astype(jnp.bfloat16)
             for j in range(n_side):
                 pair(u, i * n_side + j).start()
@@ -588,7 +633,7 @@
 
     def pair_landed(u, i):
         whole = from_partner.at[pl.ds(0, (1 + i * (n_chip - 2)) * half), unit_cols(u)]
-        remote(whole, whole, pair_send.at[0], pair_recv.at[u, i], partner).wait_recv()
+        remote(whole, whole, pair_send.at[0], pair_recv.at[sem_of(u), i], partner).wait_recv()
 
     def reduce_pair(u, chips=tuple(range(FAR, -1, -1))):
         place = unit_cols(u)
@@ -611,17 +656,19 @@
 
     def pass_on(u):
         both = from_team.at[1, :, unit_cols(u)]
-        remote(both, both, sum_send.at[0], sum_recv.at[u, 1], partner).wait_recv()
+        remote(both, both, sum_send.at[0], sum_recv.at[sem_of(u), 1], partner).wait_recv()
         for near in (2, 1):
-            at, place = chip_rows(chip_q(FAR - near, 1), c), lane_cols(u, near)
+            first, count, place = lane(u, near)
+            at, _ = lane_part(u, near, chip_q(FAR - near, 1))
+            come = from_team[1, first : first + count, place]
             part[at, place] = (
-                part[at, place].astype(jnp.float32) + from_team[1, :, place].astype(jnp.float32)
+                part[at, place].astype(jnp.float32) + come.astype(jnp.float32)
             ).astype(jnp.bfloat16)
             to_team(u, near, 2).start()
 
     def collected(u):
         rest = from_team.at[pl.ds(0, 2), :, unit_cols(u)]
-        remote(rest, rest, sum_send.at[0], sum_recv.at[u, 0], partner).wait_recv()
+        remote(rest, rest, sum_send.at[0], sum_recv.at[sem_of(u), 0], partner).wait_recv()
 
     lag = 2
 
@@ -725,26 +772,30 @@
         done = out.at[here, place]
         remote(done, done, last_sem.at[0], last_sem.at[1], partner).start()
 
+    order = tuple(range(units - 1)) + (units - 1.0, units - 0.5)
     passed = 0
-    for u in range(units):
+    for i, u in enumerate(order):
         if u == n_side:
             relay(5, 1)
         elif u % n_side == 0 and u // n_side - 1 in beyond:
             relay(5, u // n_side - 1)
-        arrived(5, line_f(u))
+        if isinstance(u, float):
+            half_landed(5, line_f(units - 1), i - units + 1)
+        else:
+            arrived(5, line_f(u))
         multiply(u, hidden, w_down)
         reduce_pair(u, (FAR,))
-        for v in range(passed, u if u > units // 2 else u - 1):
-            pass_on(v)
-            passed = v + 1
+        while passed < (i - (i < 5)) and i != units - 1:
+            pass_on(order[passed])
+            passed += 1
         reduce_pair(u, tuple(range(FAR - 1, -1, -1)))
-        if u > units // 2:
-            finish(u - units // 2 - 1)
-    for u in range(units - units // 2 - 1, units - 2):
+        if units // 2 < i < units - 1:
+            finish(order[i - units // 2 - 1])
+    for u in order[2:5]:
         finish(u)
-    pass_on(units - 1)
-    finish(units - 2)
-    finish(units - 1)
+    pass_on(order[-1])
+    for u in order[5:]:
+        finish(u)
 
     for a in range(ARRAYS):
         all_sent(block(a, 0), side_send.at[a])
@@ -831,13 +882,14 @@
         dma((2, n_chip)),
         dma((2,)),
         dma((1,)),
-        dma((units, 2)),
+        dma((units + 1, 2)),
         dma((1,)),
-        dma((units, 2)),
+        dma((units + 1, 2)),
         dma((2,)),
         dma((2, 2)),
         dma((2,)),
         dma((10,)),
+        dma((1,)),
     ]
     return pl.pallas_call(
         functools.partial(team_kernel, dims),
@@ -869,7 +921,7 @@
 
 def team_fits(mesh):
     n_rep, n_fs, n_tp = (mesh.shape[name] for name in ("rep", "fs", "tp"))
-    if n_tp != 2 or n_rep * PLANE != FAR + 1 or n_fs % PLANE:
+    if n_tp != 2 or n_rep * PLANE != FAR + 1 or n_fs % PLANE or n_fs < 3 * PLANE:
         return False
     return D % (n_fs * GDIM) == 0 and D % (n_tp * n_rep * PLANE * GDIM) == 0
 

time: 169 us -> 169 us (level)
  no operation moved by 1% of the time
where the time goes in v5:
time: 169 us
  Pallas kernels  167 us (99%)
    pallas_call x1, Pallas kernels, team_layer(): pl.pallas_call(functools.partial(team_kernel, dims), out_shape=pltpu.VMEM...  167 us

profile of v5, /device:TPU:0, one launch (start us, length us, event | category | flops | bytes accessed | tf_op | source)
XLA Modules:
  0.0 168.6 jit_solution(17449447529233865648)
XLA Ops:
  0.0 167.5 %shard_map.145 = bf16[384,2048]{1,0:T(8,128)(2,1)S(1)} custom-call(bf16[384,2048]{1,0:T(8,128)(2,1)} %tokens.1, f32[1,2048]{1,0:T(1,128)} %bitcast.4, bf16[256,1024]{1,0:T(8,128)(2,1)} %mixer_gate.1, bf16[256,1024]{1,0:T(8,128)(2,1)} %mixer_value.1, f32[1,2048]{1,0:T(1,128)} %bitcast.5, f32[1,2048]{1,0:T(1,128)} %bitcast.6, ...), custom_call_target="tpu_custom_call" | custom-call | tf_op jit(solution)/shard_map/pallas_call | solution.py:894
  167.5 1.1 copy.17

commit v6 on v5

--- a/solution.py
+++ b/solution.py
@@ -236,7 +236,7 @@
         return sources[a].at[:, pl.ds(pl.multiple_of(q * cols, cols), cols)]
 
     def own_copy(a):
-        return pltpu.make_async_copy(piece(a, q_own), block(a, f_own), own_sem.at[a])
+        return pltpu.make_async_copy(piece(a, q_own), block(a, f_own), weight_recv.at[a, f_own])
 
     q_side = x * n_side + (y + 1) % n_side
 
@@ -248,7 +248,7 @@
         return remote(
             piece(a, q_side) if a > 1 else ahead.at[a],
             block(a, f_own),
-            side_send.at[a],
+            side_send.at[0],
             weight_recv.at[a, f_own],
             (x, z * n_side + to_y, c),
         )
@@ -256,7 +256,7 @@
     def along(a, f, step, src):
         sem = up_send if step == 1 else down_send
         return remote(
-            src, block(a, f), sem.at[a], weight_recv.at[a, f], (x, f_own + step * n_side, c)
+            src, block(a, f), sem.at[a // 4], weight_recv.at[a, f], (x, f_own + step * n_side, c)
         )
 
     def halves(a, f):
@@ -267,15 +267,15 @@
         for h, ref in enumerate(halves(a, f)):
             sem = up_send if step == 1 else down_send
             recv = late_recv.at[0] if h else weight_recv.at[a, f]
-            remote(ref, ref, sem.at[a], recv, (x, f_own + step * n_side, c)).start()
+            remote(ref, ref, sem.at[a // 4], recv, (x, f_own + step * n_side, c)).start()
 
     def half_landed(a, f, h):
         ref = halves(a, f)[h]
         recv = late_recv.at[0] if h else weight_recv.at[a, f]
-        pl.when(at_end)(lambda: remote(ref, ref, side_send.at[a], recv, partner).wait_recv())
+        pl.when(at_end)(lambda: remote(ref, ref, side_send.at[0], recv, partner).wait_recv())
 
     def landed(a, f):
-        remote(block(a, f), block(a, f), side_send.at[a], weight_recv.at[a, f], partner).wait_recv()
+        remote(block(a, f), block(a, f), side_send.at[0], weight_recv.at[a, f], partner).wait_recv()
 
     def send_line(a, f, src, up=True, down=True):
         if up:
@@ -443,7 +443,7 @@
         for k in (2, 1):
             share(0, k, h, tok, tokens, c * half).start()
     tok_copy = pltpu.make_async_copy(
-        tokens, tok.at[pl.ds(pl.multiple_of(q_own * rows, rows), rows)], own_sem.at[ARRAYS]
+        tokens, tok.at[pl.ds(pl.multiple_of(q_own * rows, rows), rows)], own_sem.at[0]
     )
     tok_copy.start()
     start_side(2)
@@ -797,14 +797,16 @@
     for u in order[5:]:
         finish(u)
 
-    for a in range(ARRAYS):
-        all_sent(block(a, 0), side_send.at[a])
+    def flat(arrays, count):
+        size = sum(block(a, 0).shape[0] * block(a, 0).shape[1] for a in arrays)
+        return tok.at[pl.ds(0, count * size // width)]
+
+    all_sent(flat(range(ARRAYS), 1), side_send.at[0])
+    for i, arrays in enumerate((range(4), range(4, ARRAYS))):
         for n in range(1, n_line):
-            pl.when(z == n - 1)(lambda: all_sent(blocks_of(a, 0, n * n_side), up_send.at[a]))
+            pl.when(z == n - 1)(lambda: all_sent(flat(arrays, n * n_side), up_send.at[i]))
             pl.when(z == n)(
-                lambda: all_sent(
-                    blocks_of(a, n * n_side, (n_line - n) * n_side), down_send.at[a]
-                )
+                lambda: all_sent(flat(arrays, (n_line - n) * n_side), down_send.at[i])
             )
     all_sent(told, stat_sem.at[0])
     for g in range(2):
@@ -871,10 +873,10 @@
         pltpu.VMEM((2, cols), f32),
         pltpu.VMEM(spatial_bias.shape, f32),
         pltpu.VMEM((2, mixer_value.shape[0], cols), bf16),
-        dma((ARRAYS + 1,)),
-        dma((ARRAYS,)),
-        dma((ARRAYS,)),
-        dma((ARRAYS,)),
+        dma((1,)),
+        dma((1,)),
+        dma((2,)),
+        dma((2,)),
         dma((ARRAYS, n_fs)),
         dma((2,)),
         dma((2, 4)),

time: 169 us -> 169 us (level)
  no operation moved by 1% of the time
where the time goes in v6:
time: 169 us; the launch traced here: 168 us
  Pallas kernels  167 us (99%)
    pallas_call x1, Pallas kernels, team_layer(): pl.pallas_call(functools.partial(team_kernel, dims), out_shape=pltpu.VMEM...  167 us

profile of v6, /device:TPU:0, one launch (start us, length us, event | category | flops | bytes accessed | tf_op | source)
XLA Modules:
  0.0 168.4 jit_solution(4398949218337092178)
XLA Ops:
  0.0 167.3 %shard_map.145 = bf16[384,2048]{1,0:T(8,128)(2,1)S(1)} custom-call(bf16[384,2048]{1,0:T(8,128)(2,1)} %tokens.1, f32[1,2048]{1,0:T(1,128)} %bitcast.4, bf16[256,1024]{1,0:T(8,128)(2,1)} %mixer_gate.1, bf16[256,1024]{1,0:T(8,128)(2,1)} %mixer_value.1, f32[1,2048]{1,0:T(1,128)} %bitcast.5, f32[1,2048]{1,0:T(1,128)} %bitcast.6, ...), custom_call_target="tpu_custom_call" | custom-call | tf_op jit(solution)/shard_map/pallas_call | solution.py:896
  167.3 1.1 copy.17
